TPU v7x, 128 devices: a whole 4x4x4 slice. The times are simulated.
128 devices in a mesh: ep: 16 (over z, x), tp: 8 (over y, core).
Axes of the slice: x: 4, y: 4, z: 4, core: 2. Of those that a mesh axis runs over, the one named last changes fastest.
Arguments:
- queries: bfloat16 [32768, 2048], P('ep', 'tp'), may hold values from -128 to 128
- key_heads: bfloat16 [32768, 1024], P('ep', 'tp'), may hold values from -6 to 6
- value_heads: bfloat16 [32768, 1024], P('ep', 'tp'), may hold values from -6 to 6
- sink_logits: float32 [32], P('tp'), may hold values from 1 to 5
- mix_weight: bfloat16 [2048, 2048], replicated, may hold values from -1 to 1
- expert_input: bfloat16 [16384, 2048], P(('ep', 'tp')), may hold values from -6 to 6
- norm_gain: float32 [2048], replicated, may hold values from 0.1 to 1.9
- routes: int32 [16384, 4], P(('ep', 'tp')), may hold values from 0 to 127, all different within a row; in each aligned block of 128 rows (0 to 127, 128 to 255, ...) at most 8 rows name the same one
- route_weights: float32 [16384, 4], P(('ep', 'tp')), may hold values from 0.1 to 1
- gate_weight: bfloat16 [128, 2048, 1024], P(('ep', 'tp')), may hold values from -0.375 to 0.375
- up_weight: bfloat16 [128, 2048, 1024], P(('ep', 'tp')), may hold values from -0.375 to 0.375
- down_weight: bfloat16 [128, 1024, 2048], P(('ep', 'tp')), may hold values from -0.046875 to 0.046875
Outputs:
- mixer_out: bfloat16 [32768, 2048], P(('ep', 'tp'))
- experts_out: bfloat16 [16384, 2048], P(('ep', 'tp'))
Inputs may be any that keep to these rules, and one draw needn't show every extreme that they name: `routes`: each row names 4 different experts; within the 128 rows of one device no expert is named more than 8 times, and in some devices' rows some expert is named exactly 8 times.
All inputs are finite; a program needn't handle non-finite values.
Results may differ from a plain program's by a relative error of at most 0.012.
The roundings to bfloat16 on the way count: a program that leaves them out, or rounds other values in their place, can miss the bound.
Values may be sent and summed in bfloat16 or wider, within the bound.
A program may use at most 128 MiB of HBM per device.

v0:
```python
import math

import jax
import jax.numpy as jnp
from jax import lax
from jax.sharding import PartitionSpec as P

HEAD_DIM = 64
WINDOW = 128
GRID_W = 64


ROPE_BASE = 10000.0
CLAMP_LIMIT = 7.0
GATE_SLOPE = 1.702
NORM_EPS = 1e-05


def with_halo(cells, sides, width):
    for axis, dim in sides:
        count = lax.axis_size(axis)
        ends = count - 1
        head = lax.slice_in_dim(cells, 0, width, axis=dim)
        tail = lax.slice_in_dim(cells, cells.shape[dim] - width, cells.shape[dim], axis=dim)
        cells = jnp.concatenate(
            [
                lax.ppermute(tail, axis, [(i, (i + 1) % count) for i in range(ends)]),
                cells,
                lax.ppermute(head, axis, [((i + 1) % count, i) for i in range(ends)]),
            ],
            axis=dim,
        )
    return cells


def rotate_pairs(table, grid_rows, grid_cols, head_width):
    length = table.shape[0]
    quarter = head_width // 4
    shaped = table.reshape(length, -1, 2, 2, quarter)
    freqs = ROPE_BASE ** (-jnp.arange(0, head_width // 2, 2, dtype=jnp.float32) / (head_width // 2))
    angles = jnp.stack([grid_rows, grid_cols], axis=-1)[:, :, None] * freqs
    cosines = jnp.cos(angles)[:, None]
    sine_part = jnp.sin(angles)[:, None]
    former = shaped[..., 0, :]
    latter = shaped[..., 1, :]
    turned = jnp.stack(
        [former * cosines - latter * sine_part, latter * cosines + former * sine_part], axis=-2
    )
    return turned.reshape(length, -1)


def grid_place(positions):
    return ((positions // GRID_W).astype(jnp.float32), (positions % GRID_W).astype(jnp.float32))


def normalize(tokens_in, gain_row):
    values = tokens_in.astype(jnp.float32)
    center = jnp.mean(values, axis=-1, keepdims=True)
    spread = jnp.mean(jnp.square(values - center), axis=-1, keepdims=True)
    return ((values - center) * lax.rsqrt(spread + NORM_EPS) * gain_row).astype(jnp.bfloat16)


def expert_rows(row_block, w_gate, w_lift, w_down):
    gate_pre = jnp.dot(row_block, w_gate, preferred_element_type=jnp.float32)
    lift_pre = jnp.dot(row_block, w_lift, preferred_element_type=jnp.float32)
    gate_pre = jnp.minimum(gate_pre, CLAMP_LIMIT)
    lift_pre = jnp.clip(lift_pre, -CLAMP_LIMIT, CLAMP_LIMIT)
    activated = ((lift_pre + 1.0) * gate_pre * jax.nn.sigmoid(GATE_SLOPE * gate_pre)).astype(
        jnp.bfloat16
    )
    return jnp.dot(activated, w_down, preferred_element_type=jnp.float32).astype(jnp.bfloat16)


def body(
    queries,
    key_heads,
    value_heads,
    sink_logits,
    mix_weight,
    expert_input,
    norm_gain,
    routes,
    route_weights,
    gate_weight,
    up_weight,
    down_weight,
):
    rows_here = queries.shape[0]
    global_length = rows_here * lax.axis_size("ep")
    heads_local = sink_logits.shape[0]
    kv_local = key_heads.shape[1] // HEAD_DIM
    group_size = heads_local // kv_local
    first_global = lax.axis_index("ep") * rows_here
    positions = first_global + jnp.arange(rows_here, dtype=jnp.int32)
    grid_rows, grid_cols = grid_place(positions)
    q_rot = rotate_pairs(queries.astype(jnp.float32), grid_rows, grid_cols, HEAD_DIM).astype(
        jnp.bfloat16
    )
    k_rot = rotate_pairs(key_heads.astype(jnp.float32), grid_rows, grid_cols, HEAD_DIM).astype(
        jnp.bfloat16
    )
    paired = jnp.stack([k_rot, value_heads])
    widened = with_halo(paired, (("ep", 1),), WINDOW)
    block_rows = math.gcd(rows_here, 512)
    key_span = block_rows + 2 * WINDOW
    sink_grid = sink_logits.reshape(kv_local, group_size)

    def one_block(block_index):
        first_row = block_index * block_rows
        q_blk = lax.dynamic_slice_in_dim(q_rot, first_row, block_rows, 0)
        q_blk = q_blk.reshape(block_rows, kv_local, group_size, HEAD_DIM)
        k_blk = lax.dynamic_slice_in_dim(widened[0], first_row, key_span, 0).reshape(
            key_span, kv_local, HEAD_DIM
        )
        v_blk = lax.dynamic_slice_in_dim(widened[1], first_row, key_span, 0).reshape(
            key_span, kv_local, HEAD_DIM
        )
        q_pos = first_global + first_row + jnp.arange(block_rows, dtype=jnp.int32)
        k_pos = first_global + first_row - WINDOW + jnp.arange(key_span, dtype=jnp.int32)
        inside = (
            (jnp.abs(q_pos[:, None] - k_pos[None, :]) <= WINDOW)
            & (k_pos >= 0)
            & (k_pos < global_length)
        )
        scores = jnp.einsum(
            "qkgd,skd->kgqs", q_blk, k_blk, preferred_element_type=jnp.float32
        ) * HEAD_DIM ** (-0.5)
        scores = jnp.where(inside, scores, -jnp.inf)
        peak = jnp.maximum(jnp.max(scores, axis=-1), sink_grid[:, :, None])
        weights_exp = jnp.exp(scores - peak[..., None])
        denominator = jnp.sum(weights_exp, axis=-1) + jnp.exp(sink_grid[:, :, None] - peak)
        chances = (weights_exp / denominator[..., None]).astype(jnp.bfloat16)
        blended = jnp.einsum("kgqs,skd->qkgd", chances, v_blk, preferred_element_type=jnp.float32)
        return blended.astype(jnp.bfloat16).reshape(block_rows, heads_local * HEAD_DIM)

    blocks = lax.map(one_block, jnp.arange(rows_here // block_rows, dtype=jnp.int32))
    attended = blocks.reshape(rows_here, heads_local * HEAD_DIM)
    token_rows = lax.all_to_all(attended, "tp", split_axis=0, concat_axis=1, tiled=True)
    mixer_out = jnp.dot(token_rows, mix_weight, preferred_element_type=jnp.float32).astype(
        jnp.bfloat16
    )
    experts = lax.axis_size("ep") * lax.axis_size("tp")
    tok_local, top_count = routes.shape
    capacity = 2 * tok_local * top_count // experts
    width = expert_input.shape[1]
    normed = normalize(expert_input, norm_gain)
    flat_routes = routes.reshape(-1)
    matches = (flat_routes[:, None] == jnp.arange(experts, dtype=jnp.int32)[None, :]).astype(
        jnp.int32
    )
    earlier = jnp.cumsum(matches, axis=0) - matches
    slots = jnp.sum(earlier * matches, axis=1)
    columns = flat_routes * capacity + slots
    token_of = jnp.arange(tok_local * top_count, dtype=jnp.int32) // top_count
    table = jnp.full((experts * capacity,), tok_local, jnp.int32).at[columns].set(token_of)
    padded_in = jnp.concatenate([normed, jnp.zeros((1, width), jnp.bfloat16)], axis=0)
    outgoing = jnp.take(padded_in, table, axis=0).reshape(experts, capacity, width)
    w_gate = gate_weight[0]
    w_lift = up_weight[0]
    w_down = down_weight[0]
    arrived = lax.all_to_all(outgoing, ("ep", "tp"), split_axis=0, concat_axis=0, tiled=True)
    sources, items, feature_count = arrived.shape
    produced = expert_rows(arrived.reshape(sources * items, feature_count), w_gate, w_lift, w_down)
    produced = produced.reshape(sources, items, feature_count)
    returned = lax.all_to_all(produced, ("ep", "tp"), split_axis=0, concat_axis=0, tiled=True)
    picked = jnp.take(returned.reshape(experts * capacity, width), columns, axis=0)
    picked = picked.reshape(tok_local, top_count, width)
    summed = jnp.sum(route_weights[..., None] * picked.astype(jnp.float32), axis=1)
    return (mixer_out, summed.astype(jnp.bfloat16))


def solution(mesh):
    return jax.shard_map(
        body,
        mesh=mesh,
        in_specs=(
            P("ep", "tp"),
            P("ep", "tp"),
            P("ep", "tp"),
            P("tp"),
            P(),
            P(("ep", "tp"), None),
            P(),
            P(("ep", "tp"), None),
            P(("ep", "tp"), None),
            P(("ep", "tp"), None, None),
            P(("ep", "tp"), None, None),
            P(("ep", "tp"), None, None),
        ),
        out_specs=(P(("ep", "tp"), None), P(("ep", "tp"), None)),
        check_vma=False,
    )
```

profile of v0, /device:TPU:1, one launch (start us, length us, event | category | flops | bytes accessed | tf_op | source)
XLA Modules:
  0.0 201.1 jit_solution(13714851131860689107)
XLA Ops:
  0.7 1.3 copy.35
  2.1 1.3 copy.36
  5.3 3.9 %collective-permute-start = (bf16[2,128,128]{1,2,0:T(8,128)(2,1)}, bf16[2,128,128]{1,2,0:T(8,128)(2,1)S(1)}, u32[]{:S(2)}, u32[]{:S(2)}) collective-permute-start(bf16[2,128,128]{1,2,0:T(8,128)(2,1)} %get-tuple-element.118), channel_id=1, source_target_pairs={{0,8},{8,16},{16,24},{24,32},{32,40},{40,48},{48,56},{56,64},{64,7... | collective-permute-start | bytes 196616 | tf_op jit(solution)/shard_map/ppermute | solution.py:27
  9.3 1.3 collective-permute-start.1
  11.8 2.4 %scatter_custom_fusion = s32[1024]{0:T(1024)S(1)} fusion(s32[512]{0:T(512)S(1)} %bitcast.122, s32[512]{0:T(512)S(1)} %add_select_fusion, s32[]{:T(128)} %constant.173.clone.1), kind=kCustom, calls=%fused_computation.87 | custom fusion | bytes 4100 | tf_op jit(solution)/shard_map/scatter | solution.py:155
  15.3 6.0 %gather_fusion = bf16[1024,2048]{1,0:T(8,128)(2,1)} fusion(bf16[129,2048]{1,0:T(8,128)(2,1)S(1)} %concatenate.7, s32[1024]{0:T(1024)S(1)} %fusion.36), kind=kCustom, calls=%fused_computation | custom fusion | bytes 8392704 | tf_op jit(solution)/shard_map/jit(_take)/gather | solution.py:157
  21.3 4.7 %bitcast_select_fusion.1 = bf16[128,8,2048]{2,1,0:T(8,128)(2,1)} fusion(bf16[1024,2048]{1,0:T(8,128)(2,1)} %gather_fusion, pred[128,8]{1,0:T(8,128)(4,1)S(1)} %broadcast_in_dim.75), kind=kLoop, calls=%fused_computation.33 | loop fusion | flops 2097152 | bytes 8389632 | tf_op jit(solution)/shard_map/jit(_take)/select_n | solution.py:157
  26.0 12.6 %all-to-all-start.1 = ((bf16[128,8,2048]{2,1,0:T(8,128)(2,1)}), bf16[128,8,2048]{2,1,0:T(8,128)(2,1)}, u32[]{:S(2)}, u32[]{:S(2)}) async-start(bf16[128,8,2048]{2,1,0:T(8,128)(2,1)} %bitcast_select_fusion.1), calls=%async_computation.1 | async-start | bytes 8388608 | tf_op jit(solution)/shard_map/all_to_all | solution.py:161
  38.6 1.5 copy.37
  41.1 54.7 %while.12 = (s32[]{:T(128)}, bf16[4,512,256]{2,1,0:T(8,128)(2,1)}, bf16[2,2304,128]{1,2,0:T(8,128)(2,1)S(1)}, s32[4]{0:T(128)S(1)}, s32[]{:T(128)}, /*index=5*/b...) while((s32[]{:T(128)}, bf16[4,512,256]{2,1,0:T(8,128)(2,1)}, ...), condition=%wide.region_3.4_spmd, body=%wide.region_0.3_spmd.sunk | while | flops 423632384 | bytes 51345240 | solution.py:136
  43.3 3.9 %fusion.64 = (f32[2,2,512]{2,1,0:T(2,128)S(1)}, f32[2,768,512,2]{2,1,3,0:T(8,128)}) fusion(pred[512,768]{0,1:T(8,128)(4,1)S(1)} %fusion.63, bf16[768,2,64,1]{0,2,3,1:T(8,128)(2,1)S(1)} %bitcast.109, bf16[512,2,2,64]{0,3,2,1:T(8,128)(2,1)S(1)} %bitcast.105), kind=kOutput, calls=%fused_computation.7.clone.1 | convolution fusion | flops 206043136 | bytes 7151616 | tf_op jit(solution)/shard_map/while/body/eval_jaxpr/qkgd,skd->kgqs/dot_general | solution.py:125
  47.3 4.3 %fusion.65 = f32[2,2,512]{2,1,0:T(2,128)S(1)} fusion(f32[2,768,512,2]{2,1,3,0:T(8,128)} %get-tuple-element.181, f32[2,2,512]{2,1,0:T(2,128)S(1)} %broadcast_maximum_fusion.2, pred[512,768]{0,1:T(8,128)(4,1)S(1)} %fusion.63), kind=kLoop, calls=%fused_computation.6.clone.1 | loop fusion | flops 6289408 | bytes 6701056 | tf_op jit(solution)/shard_map/while/body/eval_jaxpr/reduce_sum | solution.py:131
  51.9 2.0 fusion.66
  57.0 3.9 %fusion.64 = (f32[2,2,512]{2,1,0:T(2,128)S(1)}, f32[2,768,512,2]{2,1,3,0:T(8,128)}) fusion(pred[512,768]{0,1:T(8,128)(4,1)S(1)} %fusion.63, bf16[768,2,64,1]{0,2,3,1:T(8,128)(2,1)S(1)} %bitcast.109, bf16[512,2,2,64]{0,3,2,1:T(8,128)(2,1)S(1)} %bitcast.105), kind=kOutput, calls=%fused_computation.7.clone.1 | convolution fusion | flops 206043136 | bytes 7151616 | tf_op jit(solution)/shard_map/while/body/eval_jaxpr/qkgd,skd->kgqs/dot_general | solution.py:125
  61.0 4.3 %fusion.65 = f32[2,2,512]{2,1,0:T(2,128)S(1)} fusion(f32[2,768,512,2]{2,1,3,0:T(8,128)} %get-tuple-element.181, f32[2,2,512]{2,1,0:T(2,128)S(1)} %broadcast_maximum_fusion.2, pred[512,768]{0,1:T(8,128)(4,1)S(1)} %fusion.63), kind=kLoop, calls=%fused_computation.6.clone.1 | loop fusion | flops 6289408 | bytes 6701056 | tf_op jit(solution)/shard_map/while/body/eval_jaxpr/reduce_sum | solution.py:131
  65.5 2.0 fusion.66
  70.6 3.9 %fusion.64 = (f32[2,2,512]{2,1,0:T(2,128)S(1)}, f32[2,768,512,2]{2,1,3,0:T(8,128)}) fusion(pred[512,768]{0,1:T(8,128)(4,1)S(1)} %fusion.63, bf16[768,2,64,1]{0,2,3,1:T(8,128)(2,1)S(1)} %bitcast.109, bf16[512,2,2,64]{0,3,2,1:T(8,128)(2,1)S(1)} %bitcast.105), kind=kOutput, calls=%fused_computation.7.clone.1 | convolution fusion | flops 206043136 | bytes 7151616 | tf_op jit(solution)/shard_map/while/body/eval_jaxpr/qkgd,skd->kgqs/dot_general | solution.py:125
  74.7 4.3 %fusion.65 = f32[2,2,512]{2,1,0:T(2,128)S(1)} fusion(f32[2,768,512,2]{2,1,3,0:T(8,128)} %get-tuple-element.181, f32[2,2,512]{2,1,0:T(2,128)S(1)} %broadcast_maximum_fusion.2, pred[512,768]{0,1:T(8,128)(4,1)S(1)} %fusion.63), kind=kLoop, calls=%fused_computation.6.clone.1 | loop fusion | flops 6289408 | bytes 6701056 | tf_op jit(solution)/shard_map/while/body/eval_jaxpr/reduce_sum | solution.py:131
  79.2 2.0 fusion.66
  84.3 3.9 %fusion.64 = (f32[2,2,512]{2,1,0:T(2,128)S(1)}, f32[2,768,512,2]{2,1,3,0:T(8,128)}) fusion(pred[512,768]{0,1:T(8,128)(4,1)S(1)} %fusion.63, bf16[768,2,64,1]{0,2,3,1:T(8,128)(2,1)S(1)} %bitcast.109, bf16[512,2,2,64]{0,3,2,1:T(8,128)(2,1)S(1)} %bitcast.105), kind=kOutput, calls=%fused_computation.7.clone.1 | convolution fusion | flops 206043136 | bytes 7151616 | tf_op jit(solution)/shard_map/while/body/eval_jaxpr/qkgd,skd->kgqs/dot_general | solution.py:125
  88.3 4.3 %fusion.65 = f32[2,2,512]{2,1,0:T(2,128)S(1)} fusion(f32[2,768,512,2]{2,1,3,0:T(8,128)} %get-tuple-element.181, f32[2,2,512]{2,1,0:T(2,128)S(1)} %broadcast_maximum_fusion.2, pred[512,768]{0,1:T(8,128)(4,1)S(1)} %fusion.63), kind=kLoop, calls=%fused_computation.6.clone.1 | loop fusion | flops 6289408 | bytes 6701056 | tf_op jit(solution)/shard_map/while/body/eval_jaxpr/reduce_sum | solution.py:131
  92.9 2.0 fusion.66
  95.7 4.8 %all-to-all-start = ((bf16[8,256,256]{2,1,0:T(8,128)(2,1)}), bf16[8,256,256]{2,1,0:T(8,128)(2,1)S(1)}, u32[]{:S(2)}, u32[]{:S(2)}) async-start(bf16[8,256,256]{2,1,0:T(8,128)(2,1)} %bitcast.118), calls=%async_computation | async-start | bytes 2097152 | tf_op jit(solution)/shard_map/all_to_all | solution.py:138
  100.5 7.6 %fusion.12 = f32[1024,1024]{1,0:T(8,128)S(1)} fusion(bf16[1,2048,1024]{2,1,0:T(8,128)(2,1)} %param.23, bf16[128,8,2048]{2,1,0:T(8,128)(2,1)} %all-to-all-done.1), kind=kOutput, calls=%fused_computation.27 | convolution fusion | flops 4294967296 | bytes 12582912 | tf_op jit(solution)/shard_map/dot_general | solution.py:64
  108.2 8.0 %multiply_convert_fusion = bf16[1024,1024]{1,0:T(8,128)(2,1)S(1)} fusion(f32[1024,1024]{1,0:T(8,128)S(1)} %fusion.12, bf16[1,2048,1024]{2,1,0:T(8,128)(2,1)S(1)} %copy-done.9, bf16[128,8,2048]{2,1,0:T(8,128)(2,1)} %all-to-all-done.1), kind=kOutput, calls=%fused_computation.36 | convolution fusion | flops 4305453056 | bytes 14680064 | tf_op jit(solution)/shard_map/dot_general | solution.py:65
  116.3 6.1 %convert_bitcast_fusion = bf16[128,8,2048]{2,1,0:T(8,128)(2,1)} fusion(bf16[1024,1024]{1,0:T(8,128)(2,1)S(1)} %multiply_convert_fusion, bf16[1,1024,2048]{2,1,0:T(8,128)(2,1)S(1)} %copy-done.10), kind=kOutput, calls=%fused_computation.35 | convolution fusion | flops 4297064448 | bytes 10485760 | tf_op jit(solution)/shard_map/dot_general | solution.py:71
  122.3 10.2 %all-to-all-start.2 = ((bf16[128,8,2048]{2,1,0:T(8,128)(2,1)}), bf16[128,8,2048]{2,1,0:T(8,128)(2,1)}, u32[]{:S(2)}, u32[]{:S(2)}) async-start(bf16[128,8,2048]{2,1,0:T(8,128)(2,1)} %convert_bitcast_fusion), calls=%async_computation.2 | async-start | bytes 8388608 | tf_op jit(solution)/shard_map/all_to_all | solution.py:165
  133.6 6.7 %convolution_convert_fusion = bf16[256,2048]{1,0:T(8,128)(2,1)} fusion(bf16[256,2048]{0,1:T(8,128)(2,1)S(1)} %bitcast.104, bf16[2048,2048]{1,0:T(8,128)(2,1)} %param.18), kind=kOutput, calls=%fused_computation.37 | convolution fusion | flops 2148007936 | bytes 10485760 | tf_op jit(solution)/shard_map/dot_general | solution.py:139
  140.3 45.0 %all-to-all-done.2 = bf16[128,8,2048]{2,1,0:T(8,128)(2,1)} async-done(((bf16[128,8,2048]{2,1,0:T(8,128)(2,1)}), bf16[128,8,2048]{2,1,0:T(8,128)(2,1)}, u32[]{:S(2)}, u32[]{:S(2)}) %all-to-all-start.2) | async-done | bytes 4194336 | tf_op jit(solution)/shard_map/all_to_all | solution.py:165
  185.3 7.1 %gather_fusion.1 = bf16[512,2048]{1,0:T(8,128)(2,1)S(1)} fusion(bf16[1024,2048]{1,0:T(8,128)(2,1)} %bitcast.32, s32[1024]{0:T(1024)S(1)} %pad_clamp_fusion), kind=kCustom, calls=%fused_computation.1 | custom fusion | bytes 4196352 | tf_op jit(solution)/shard_map/jit(_take)/gather | solution.py:166
  192.4 2.2 %gather.15 = bf16[128,4,2048]{2,1,0:T(4,128)(2,1)} reshape(bf16[512,2048]{1,0:T(8,128)(2,1)S(1)} %gather_fusion.1) | data formatting | bytes 4194304 | tf_op jit(solution)/shard_map/jit(_take)/gather | solution.py:166
  194.6 6.4 %multiply_reduce_fusion = bf16[128,2048]{1,0:T(8,128)(2,1)} fusion(bf16[128,4,2048]{2,1,0:T(4,128)(2,1)} %gather.15, f32[128,4]{1,0:T(8,128)S(1)} %copy.40, pred[128,4]{1,0:T(8,128)(4,1)S(1)} %copy.46), kind=kLoop, calls=%fused_computation.34 | loop fusion | flops 3932160 | bytes 2624000 | tf_op jit(solution)/shard_map/reduce_sum | solution.py:168
  (133 shorter events, 17.2 us)
Async XLA Ops:
  0.7 9.8 %copy-start.6 = (s32[128,4]{0,1:T(4,128)S(1)}, s32[128,4]{0,1:T(4,128)}, u32[]{:S(2)}) copy-start(s32[128,4]{0,1:T(4,128)} %param.21) | copy-start | bytes 6148
  2.1 12.2 %copy-start.1 = (bf16[128,2048]{1,0:T(8,128)(2,1)S(1)}, bf16[128,2048]{1,0:T(8,128)(2,1)}, u32[]{:S(2)}) copy-start(bf16[128,2048]{1,0:T(8,128)(2,1)} %param.19) | copy-start | bytes 1572868
  3.4 11.5 %copy-start.7 = (f32[2048]{0:T(1024)S(1)}, f32[2048]{0:T(1024)}, u32[]{:S(2)}) copy-start(f32[2048]{0:T(1024)} %param.20) | copy-start | bytes 24580
  4.5 10.4 %copy-start.2 = (f32[2048,2,16]{0,2,1:T(8,128)}, f32[2048,2,16]{0,2,1:T(8,128)S(1)}, u32[]{:S(2)}) copy-start(f32[2048,2,16]{0,2,1:T(8,128)S(1)} %get-tuple-element.120) | copy-start | bytes 786436
  4.5 10.8 %copy-start.4 = (f32[2048,2,16]{0,2,1:T(8,128)}, f32[2048,2,16]{0,2,1:T(8,128)S(1)}, u32[]{:S(2)}) copy-start(f32[2048,2,16]{0,2,1:T(8,128)S(1)} %get-tuple-element.121) | copy-start | bytes 786436
  5.3 35.5 %collective-permute-start = (bf16[2,128,128]{1,2,0:T(8,128)(2,1)}, bf16[2,128,128]{1,2,0:T(8,128)(2,1)S(1)}, u32[]{:S(2)}, u32[]{:S(2)}) collective-permute-start(bf16[2,128,128]{1,2,0:T(8,128)(2,1)} %get-tuple-element.118), channel_id=1, source_target_pairs={{0,8},{8,16},{16,24},{24,32},{32,40},{40,48},{48,56},{56,64},{64,7... | collective-permute-start | bytes 196616 | tf_op jit(solution)/shard_map/ppermute | solution.py:27
  9.3 31.6 %collective-permute-start.1 = (bf16[2,128,128]{1,2,0:T(8,128)(2,1)S(1)}, bf16[2,128,128]{1,2,0:T(8,128)(2,1)S(1)}, u32[]{:S(2)}, u32[]{:S(2)}) collective-permute-start(bf16[2,128,128]{1,2,0:T(8,128)(2,1)S(1)} %get-tuple-element.119), channel_id=1, source_target_pairs={{8,0},{16,8},{24,16},{32,24},{40,32},{48,40},{56,48},{64,56},{72,6... | collective-permute-start | bytes 196616 | tf_op jit(solution)/shard_map/ppermute | solution.py:29
  26.0 69.7 %all-to-all-start.1 = ((bf16[128,8,2048]{2,1,0:T(8,128)(2,1)}), bf16[128,8,2048]{2,1,0:T(8,128)(2,1)}, u32[]{:S(2)}, u32[]{:S(2)}) async-start(bf16[128,8,2048]{2,1,0:T(8,128)(2,1)} %bitcast_select_fusion.1), calls=%async_computation.1 | async-start | bytes 8388608 | tf_op jit(solution)/shard_map/all_to_all | solution.py:161
  38.6 1.8 copy-start.3
  38.6 1.8 copy-start.5
  40.4 0.7 copy-start.11
  47.3 4.6 %copy-start = (f32[2,768,512,2]{2,1,3,0:T(8,128)S(1)}, f32[2,768,512,2]{2,1,3,0:T(8,128)}, u32[]{:S(2)}) copy-start(f32[2,768,512,2]{2,1,3,0:T(8,128)} %get-tuple-element.181) | copy-start | bytes 18874372 | tf_op jit(solution)/shard_map/while
  60.9 4.6 %copy-start = (f32[2,768,512,2]{2,1,3,0:T(8,128)S(1)}, f32[2,768,512,2]{2,1,3,0:T(8,128)}, u32[]{:S(2)}) copy-start(f32[2,768,512,2]{2,1,3,0:T(8,128)} %get-tuple-element.181) | copy-start | bytes 18874372 | tf_op jit(solution)/shard_map/while
  74.6 4.6 %copy-start = (f32[2,768,512,2]{2,1,3,0:T(8,128)S(1)}, f32[2,768,512,2]{2,1,3,0:T(8,128)}, u32[]{:S(2)}) copy-start(f32[2,768,512,2]{2,1,3,0:T(8,128)} %get-tuple-element.181) | copy-start | bytes 18874372 | tf_op jit(solution)/shard_map/while
  88.3 4.6 %copy-start = (f32[2,768,512,2]{2,1,3,0:T(8,128)S(1)}, f32[2,768,512,2]{2,1,3,0:T(8,128)}, u32[]{:S(2)}) copy-start(f32[2,768,512,2]{2,1,3,0:T(8,128)} %get-tuple-element.181) | copy-start | bytes 18874372 | tf_op jit(solution)/shard_map/while
  95.7 26.6 %all-to-all-start = ((bf16[8,256,256]{2,1,0:T(8,128)(2,1)}), bf16[8,256,256]{2,1,0:T(8,128)(2,1)S(1)}, u32[]{:S(2)}, u32[]{:S(2)}) async-start(bf16[8,256,256]{2,1,0:T(8,128)(2,1)} %bitcast.118), calls=%async_computation | async-start | bytes 2097152 | tf_op jit(solution)/shard_map/all_to_all | solution.py:138
  100.5 7.7 %copy-start.9 = (bf16[1,2048,1024]{2,1,0:T(8,128)(2,1)S(1)}, bf16[1,2048,1024]{2,1,0:T(8,128)(2,1)}, u32[]{:S(2)}) copy-start(bf16[1,2048,1024]{2,1,0:T(8,128)(2,1)} %param.24) | copy-start | bytes 12582916
  108.2 8.0 %copy-start.10 = (bf16[1,1024,2048]{2,1,0:T(8,128)(2,1)S(1)}, bf16[1,1024,2048]{2,1,0:T(8,128)(2,1)}, u32[]{:S(2)}) copy-start(bf16[1,1024,2048]{2,1,0:T(8,128)(2,1)} %param.25) | copy-start | bytes 12582916
  122.3 10.6 %copy-start.8 = (f32[128,4]{0,1:T(4,128)S(1)}, f32[128,4]{0,1:T(4,128)}, u32[]{:S(2)}) copy-start(f32[128,4]{0,1:T(4,128)} %param.22) | copy-start | bytes 6148
  122.3 62.9 %all-to-all-start.2 = ((bf16[128,8,2048]{2,1,0:T(8,128)(2,1)}), bf16[128,8,2048]{2,1,0:T(8,128)(2,1)}, u32[]{:S(2)}, u32[]{:S(2)}) async-start(bf16[128,8,2048]{2,1,0:T(8,128)(2,1)} %convert_bitcast_fusion), calls=%async_computation.2 | async-start | bytes 8388608 | tf_op jit(solution)/shard_map/all_to_all | solution.py:165
where the time goes:
time: 202 us; the launch traced here: 201 us
  matrix products  52 us (26%)
  waiting for transfers between devices  45 us (22%)
  other arithmetic  36.1 us (18%)
  starting transfers between devices  32.8 us (16%)
  local copies, waits for them, and re-layouts  31.1 us (15%)
  loops' own time  2.87 us (1%)
    all_to_all x1, waiting for transfers between devices, body(): lax.all_to_all(produced, ('ep', 'tp'), split_axis=0, concat_axis=0, tiled...  45 us
    reduce_sum x4, other arithmetic, one_block(): jnp.sum(weights_exp, axis=-1) + jnp.exp(sink_grid[:, :, None] - peak)  17.1 us
    dot_general x4, matrix products, one_block(): jnp.einsum('qkgd,skd->kgqs', q_blk, k_blk, preferred_element_type=jnp.flo...  15.6 us
    all_to_all x1, starting transfers between devices, body(): lax.all_to_all(outgoing, ('ep', 'tp'), split_axis=0, concat_axis=0, tiled...  12.6 us
    all_to_all x1, starting transfers between devices, body(): lax.all_to_all(produced, ('ep', 'tp'), split_axis=0, concat_axis=0, tiled...  10.2 us
    gather x2, local copies, waits for them, and re-layouts, body(): jnp.take(returned.reshape(experts * capacity, width), columns, axis=0)  9.35 us
    dot_general x1, matrix products, expert_rows(): lift_pre = jnp.dot(row_block, w_lift, preferred_element_type=jnp.float32)  8.03 us
    dot_general x4, matrix products, one_block(): jnp.einsum('kgqs,skd->qkgd', chances, v_blk, preferred_element_type=jnp.f...  7.98 us
  transfers between devices with their start and end apart: 5, of which 1 were waited for; matrix products, arithmetic and copies ran while one was open for 49% of the time, Pallas kernels for 0%

commit v1 on v0

v1 whole, which is shorter than its diff:
```python
import functools
import math

import jax
import jax.numpy as jnp
import numpy as np
from jax import lax
from jax.experimental import pallas as pl
from jax.experimental.pallas import tpu as pltpu
from jax.sharding import PartitionSpec as P

MESH = pl.DeviceIdType.MESH
BF16 = jnp.bfloat16
F32 = jnp.float32
GRID_W = 64
ROPE_BASE = 10000.0
CLAMP_LIMIT = 7.0
GATE_SLOPE = 1.702
NORM_EPS = 1e-05
BASE = (0, 1024, 1536)
COLS = (512, 256, 256)
AXES = (0, 1, 2)


def rope_tables():
    freqs = np.float32(ROPE_BASE) ** (-np.arange(0, 32, 2, dtype=np.float32) / np.float32(32))
    lane = np.arange(128)
    by_row = (lane % 64) < 32
    freq = freqs[lane % 16].astype(np.float32)
    rows = np.clip(np.arange(-2, 514), 0, None).astype(np.float32)
    cols = np.arange(64).astype(np.float32)
    row_angle = (rows[:, None] * freq).astype(np.float32).astype(np.float64)
    col_angle = (cols[:, None] * freq).astype(np.float32).astype(np.float64)
    row_cos = np.where(by_row, np.cos(row_angle), 0.0).astype(np.float32)[:, None, :]
    row_sin = np.where(by_row, np.sin(row_angle), 0.0).astype(np.float32)[:, None, :]
    col_cos = np.where(by_row, 0.0, np.cos(col_angle)).astype(np.float32)
    col_sin = np.where(by_row, 0.0, np.sin(col_angle)).astype(np.float32)
    pairs = np.zeros((256, 256), np.float32)
    for l in range(256):
        if l % 32 < 16:
            pairs[l + 16, l] = -1.0
        else:
            pairs[l - 16, l] = 1.0
    return row_cos, row_sin, col_cos, col_sin, pairs


def device(z, x, y, c):
    return (z * 4 + x, y * 2 + c)


def wrap4(v):
    return lax.rem(v, 4)


def aligned(v, n=128):
    return pl.multiple_of(v, n)


def dot(a, b):
    return jnp.dot(a, b, preferred_element_type=F32)


def kernel(
    sink_ref, x_ref, gain_ref, meta_ref, pairs_ref, col_cos_ref, col_sin_ref,
    row_cos_hbm, row_sin_hbm, q_hbm, k_hbm, v_hbm, mix_hbm, wg_hbm, wu_hbm, wd_hbm,
    mo_ref, eo_ref,
    q, kx, vx, krot, kswap, vswap, att, att_in, row_cos, row_sin, mix, wg, wu, wd,
    nrm, metas, ag_y, ag_x, ag_z, pk_y, pk_x, pk_z, arr, act, prod, ret_y, ret_x, ret_z,
    mixing, rs_y, rs_x, rs_z, own_meta, dummy,
    load_sem, halo_send, halo_recv, meta_send, meta_recv, ag_send, ag_recv,
    pk_send, y_recv, x_recv, z_recv, att_send, att_recv, ret_send, ret_recv, rs_send, rs_recv,
):
    ep, tp = lax.axis_index("ep"), lax.axis_index("tp")
    z, x, y, c = ep // 4, lax.rem(ep, 4), tp // 2, lax.rem(tp, 2)
    ag, pk, ret, rs = (ag_y, ag_x, ag_z), (pk_y, pk_x, pk_z), (ret_y, ret_x, ret_z), (rs_y, rs_x, rs_z)

    barrier = pltpu.get_barrier_semaphore()
    peers = 0
    for dz in range(4):
        for dx in range(4):
            for dy in range(4):
                for dc in range(2):
                    if (dz and dx and dy) or not (dz or dx or dy or dc):
                        continue
                    peers += 1
                    pl.semaphore_signal(
                        barrier, 1, device_id=device(wrap4(z + dz), wrap4(x + dx), wrap4(y + dy), c ^ dc),
                        device_id_type=MESH,
                    )

    loads = [
        pltpu.make_async_copy(k_hbm, kx.at[pl.ds(128, 2048)], load_sem.at[0]),
        pltpu.make_async_copy(v_hbm, vx.at[pl.ds(128, 2048)], load_sem.at[1]),
        pltpu.make_async_copy(q_hbm, q, load_sem.at[2]),
        pltpu.make_async_copy(row_cos_hbm.at[pl.ds(ep * 32, 36)], row_cos, load_sem.at[3]),
        pltpu.make_async_copy(row_sin_hbm.at[pl.ds(ep * 32, 36)], row_sin, load_sem.at[4]),
        pltpu.make_async_copy(wg_hbm.at[0], wg, load_sem.at[5]),
        pltpu.make_async_copy(wu_hbm.at[0], wu, load_sem.at[6]),
        pltpu.make_async_copy(wd_hbm.at[0], wd, load_sem.at[7]),
        pltpu.make_async_copy(mix_hbm, mix, load_sem.at[8]),
    ]
    for copy in loads:
        copy.start()

    values = x_ref[...].astype(F32)
    center = jnp.mean(values, axis=-1, keepdims=True)
    moved = values - center
    spread = jnp.mean(jnp.square(moved), axis=-1, keepdims=True)
    nrm[...] = (moved * lax.rsqrt(spread + NORM_EPS) * gain_ref[...]).astype(BF16)
    expert_of = lax.broadcasted_iota(jnp.int32, (128, 128), 0).astype(F32)
    routes = [meta_ref[k : k + 1, :] for k in range(4)]
    named = [(expert_of == routes[k]).astype(F32) for k in range(4)]
    named_any = named[0] + named[1] + named[2] + named[3]
    earlier = (
        lax.broadcasted_iota(jnp.int32, (128, 128), 0) < lax.broadcasted_iota(jnp.int32, (128, 128), 1)
    ).astype(BF16)
    before = dot(named_any.astype(BF16), earlier)
    core = c.astype(F32)
    for k in range(4):
        slot = jnp.sum(before * named[k], axis=0, keepdims=True)
        own_meta[k : k + 1, :] = routes[k] * 16.0 + core * 8.0 + slot
    own_meta[4:8, :] = meta_ref[4:8, :]

    pl.semaphore_wait(barrier, peers)

    def line_peer(axis, j, cc):
        if axis == 0:
            return device(z, x, j, cc)
        if axis == 1:
            return device(z, j, y, cc)
        return device(j, x, y, cc)

    line_pos = (y, x, z)

    def remote(src, dst, ssem, rsem, target):
        pltpu.make_async_remote_copy(
            src_ref=src, dst_ref=dst, send_sem=ssem, recv_sem=rsem, device_id=target, device_id_type=MESH
        ).start()

    def drain(ref, sem):
        pltpu.make_async_copy(ref, ref, sem).wait()

    line_steps = [(0, 1), (1, 0), (1, 1), (3, 0), (3, 1), (2, 0), (2, 1)]
    for axis in AXES:
        for step, dc in line_steps:
            j = wrap4(line_pos[axis] + step)
            remote(
                own_meta, metas.at[axis, line_pos[axis], :, pl.ds(aligned(c * 128), 128)],
                meta_send, meta_recv, line_peer(axis, j, c ^ dc),
            )
    for axis in (2, 1, 0):
        for step, dc in line_steps:
            j = wrap4(line_pos[axis] + step)
            cc = c ^ dc
            first = aligned(BASE[axis] + cc * COLS[axis])
            remote(
                nrm.at[:, pl.ds(first, COLS[axis])], ag[axis].at[line_pos[axis], c],
                ag_send.at[axis], ag_recv.at[axis], line_peer(axis, j, cc),
            )
    after, ahead = lax.rem(ep + 1, 16), lax.rem(ep + 15, 16)
    for n, (src, dst) in enumerate(((k_hbm, kx), (v_hbm, vx))):
        remote(
            src.at[pl.ds(1920, 128)], dst.at[pl.ds(0, 128)], halo_send.at[2 * n], halo_recv.at[2 * n], (after, tp)
        )
        remote(
            src.at[pl.ds(0, 128)], dst.at[pl.ds(2176, 128)], halo_send.at[2 * n + 1], halo_recv.at[2 * n + 1],
            (ahead, tp),
        )
    for axis in AXES:
        first = aligned(BASE[axis] + c * COLS[axis])
        ag[axis][line_pos[axis], c] = nrm[:, pl.ds(first, COLS[axis])]
        metas[axis, line_pos[axis], :, pl.ds(aligned(c * 128), 128)] = own_meta[...]

    def plane_expert(axis, e):
        if axis == 0:
            return (e // 2) * 8 + y * 2 + lax.rem(e, 2)
        if axis == 1:
            return (e // 8) * 32 + x * 8 + lax.rem(e, 8)
        return z * 32 + e

    drain(dummy, meta_recv)
    self_at = ((z * 4 + x) * 2 + c, (z * 4 + y) * 2 + c, (x * 4 + y) * 2 + c)

    def pack(axis):
        drain(ag[axis].at[:, :, pl.ds(0, 112), :], ag_recv.at[axis])
        r = lax.broadcasted_iota(jnp.int32, (512, 256), 0)
        key = (plane_expert(axis, r // 16) * 16 + lax.rem(r, 16)).astype(F32)

        def one(j, carry):
            hit = key == metas[axis, j, 0:1, :]
            for k in range(1, 4):
                hit = hit | (key == metas[axis, j, k : k + 1, :])
            rows = ag[axis][j].reshape(256, COLS[axis])
            packed = dot(hit.astype(F32).astype(BF16), rows).astype(BF16)
            pk[axis][:, j] = packed.reshape(32, 16, COLS[axis])
            return carry

        lax.fori_loop(0, 4, one, 0)

    def cols_of(axis, cc):
        return pl.ds(aligned(BASE[axis] + cc * COLS[axis]), COLS[axis])

    pack(2)
    for dx, dy, dc in [(a, b, d) for a in range(4) for b in range(4) for d in range(2)]:
        xt, yt, ct = wrap4(x + dx), wrap4(y + dy), c ^ dc
        if dx or dy or dc:
            remote(
                pk_z.at[(xt * 4 + yt) * 2 + ct], arr.at[:, x, y, :, cols_of(2, c)],
                pk_send.at[2], z_recv, device(z, xt, yt, ct),
            )
    arr[:, x, y, :, cols_of(2, c)] = pk_z[self_at[2]]
    pack(1)
    for dz, dy, dc in [(a, b, d) for a in range(4) for b in range(4) for d in range(2)]:
        zt, yt, ct = wrap4(z + dz), wrap4(y + dy), c ^ dc
        if dz or dy or dc:
            remote(
                pk_x.at[(zt * 4 + yt) * 2 + ct], arr.at[z, :, y, :, cols_of(1, c)],
                pk_send.at[1], x_recv.at[dz], device(zt, x, yt, ct),
            )
    arr[z, :, y, :, cols_of(1, c)] = pk_x[self_at[1]]
    pack(0)
    for dz, dx, dc in [(a, b, d) for a in range(4) for b in range(4) for d in range(2)]:
        zt, xt, ct = wrap4(z + dz), wrap4(x + dx), c ^ dc
        if dz or dx or dc:
            remote(
                pk_y.at[(zt * 4 + xt) * 2 + ct], arr.at[z, x, :, :, cols_of(0, c)],
                pk_send.at[0], y_recv.at[dz], device(zt, xt, y, ct),
            )
    arr[z, x, :, :, cols_of(0, c)] = pk_y[self_at[0]]

    for copy in loads[:5]:
        copy.wait()
    drain(kx.at[pl.ds(0, 128)], halo_recv.at[0])
    drain(kx.at[pl.ds(2176, 128)], halo_recv.at[1])
    drain(vx.at[pl.ds(0, 128)], halo_recv.at[2])
    drain(vx.at[pl.ds(2176, 128)], halo_recv.at[3])
    low = lax.rem(lax.broadcasted_iota(jnp.int32, (128, 128), 1), 128) < 64

    def turn_tables(g):
        cs = row_cos[pl.ds(g, 2)] + col_cos_ref[...][None]
        sn = row_sin[pl.ds(g, 2)] + col_sin_ref[...][None]
        return cs.reshape(128, 128), sn.reshape(128, 128)

    def turn_keys(b, carry):
        at = pl.ds(aligned(b * 128), 128)
        cs, sn = turn_tables(b * 2)
        kb = kx[at, :]
        turned = kb.astype(F32) * cs + dot(kb, pairs_ref[0:128, 0:128]) * sn
        krot[at, :] = turned.astype(BF16)
        kswap[at, :] = pltpu.roll(turned, 64, 1).astype(BF16)
        vswap[at, :] = pltpu.roll(vx[at, :].astype(F32), 64, 1).astype(BF16)
        return carry

    lax.fori_loop(0, 18, turn_keys, 0)
    i_at = lax.broadcasted_iota(jnp.int32, (256, 128), 0)
    i_at = lax.rem(i_at, 128)
    j_at = lax.broadcasted_iota(jnp.int32, (256, 128), 1)
    gap = j_at - i_at
    upper = lax.broadcasted_iota(jnp.int32, (256, 1), 0) < 128

    def attend(b):
        cs, sn = turn_tables(b * 2 + 2)
        cs = jnp.concatenate([cs, cs], axis=1)
        sn = jnp.concatenate([sn, sn], axis=1)
        qb = q[pl.ds(aligned(b * 128), 128), :]
        qr = (qb.astype(F32) * cs + dot(qb, pairs_ref[...]) * sn) * 0.125
        q01, q23 = qr[:, :128], qr[:, 128:]
        span = pl.ds(aligned(b * 128), 384)
        least = jnp.where((ep == 0) & (b == 0), 1000, 0)
        most = jnp.where((ep == 15) & (b == 15), -1000, 0)

        def pair(q_two, keys, vals, sink):
            s = lax.dot_general(
                q_two.astype(BF16), keys[span, :], (((1,), (1,)), ((), ())), preferred_element_type=F32
            )
            s0 = jnp.where(gap >= least, s[:, :128], -1e30)
            s1 = s[:, 128:256]
            s2 = jnp.where(gap <= most, s[:, 256:], -1e30)
            peak = jnp.maximum(
                jnp.max(jnp.maximum(jnp.maximum(s0, s1), s2), axis=1, keepdims=True), sink
            )
            e0, e1, e2 = jnp.exp(s0 - peak), jnp.exp(s1 - peak), jnp.exp(s2 - peak)
            total = jnp.sum(e0 + e1 + e2, axis=1, keepdims=True) + jnp.exp(sink - peak)
            inv = 1.0 / total
            p = jnp.concatenate([(e * inv).astype(BF16) for e in (e0, e1, e2)], axis=1)
            return dot(p, vals[span, :])

        oa = pair(
            jnp.concatenate([jnp.where(low, q01, 0.0), jnp.where(low, 0.0, q23)], axis=0), krot, vx,
            jnp.where(upper, sink_ref[0], sink_ref[3]),
        )
        ob = pair(
            jnp.concatenate([jnp.where(low, 0.0, q01), jnp.where(low, q23, 0.0)], axis=0), kswap, vswap,
            jnp.where(upper, sink_ref[1], sink_ref[2]),
        )
        out = jnp.concatenate(
            [jnp.where(low, oa[:128], ob[:128]), jnp.where(low, ob[128:], oa[128:])], axis=1
        )
        att[pl.ds(aligned(b * 128), 128), :] = out.astype(BF16)

    def attend_for(s, carry):
        t = lax.rem(tp + 1 + s, 8)

        def half(h, inner):
            attend(t * 2 + h)
            return inner

        lax.fori_loop(0, 2, half, 0)
        here = att.at[pl.ds(aligned(t * 256, 256), 256)]

        @pl.when(s < 7)
        def _():
            remote(here, att_in.at[:, pl.ds(aligned(tp * 256), 256)], att_send, att_recv, (ep, t))

        return carry

    lax.fori_loop(0, 8, attend_for, 0)
    att_in[:, pl.ds(aligned(tp * 256), 256)] = att[pl.ds(aligned(tp * 256, 256), 256), :]

    for axis in AXES:
        r = lax.broadcasted_iota(jnp.int32, (256, 512), 1)
        key = (plane_expert(axis, r // 16) * 16 + lax.rem(r, 16)).astype(F32)

        def weigh(j, carry):
            turned = jnp.transpose(metas[axis, j])
            share = jnp.zeros((256, 512), F32)
            for k in range(4):
                share += jnp.where(key == turned[:, k : k + 1], turned[:, 4 + k : 5 + k], 0.0)
            mixing[axis, j] = share.astype(BF16)
            return carry

        lax.fori_loop(0, 4, weigh, 0)

    for copy in loads[5:8]:
        copy.wait()
    drain(pk_z.at[pl.ds(0, 31)], z_recv)

    for dz in range(4):
        zs = wrap4(z + 4 - dz)
        if dz == 0:
            drain(arr.at[0, :, :, :, pl.ds(0, 896)], y_recv.at[0])
            drain(arr.at[0, pl.ds(0, 2), :, :, pl.ds(0, 896)], x_recv.at[0])
        else:
            drain(arr.at[0, :, :, :, pl.ds(0, 1024)], y_recv.at[dz])
            drain(arr.at[0, :, :, :, pl.ds(0, 512)], x_recv.at[dz])

        def hidden(f, carry):
            at = pl.ds(aligned(f * 256, 256), 256)
            rows = arr[zs].reshape(256, 2048)
            gate = jnp.minimum(dot(rows, wg[:, at]), CLAMP_LIMIT)
            lift = jnp.clip(dot(rows, wu[:, at]), -CLAMP_LIMIT, CLAMP_LIMIT)
            act[:, at] = ((lift + 1.0) * gate * jax.nn.sigmoid(GATE_SLOPE * gate)).astype(BF16)
            return carry

        lax.fori_loop(0, 4, hidden, 0)

        def down(f, carry):
            at = pl.ds(aligned(f * 256, 256), 256)
            res = dot(act[...], wd[:, at]).astype(BF16)
            prod[zs, :, :, :, at] = res.reshape(4, 4, 16, 256)
            return carry

        lax.fori_loop(0, 8, down, 0)

        for d1 in range(4):
            for dc in range(2):
                xt, yt, ct = wrap4(x + d1), wrap4(y + d1), c ^ dc
                if dz or d1 or dc:
                    remote(
                        prod.at[zs, xt, :, :, cols_of(0, ct)], ret_y.at[self_at[0]],
                        ret_send.at[0], ret_recv.at[0], device(zs, xt, y, ct),
                    )
                    remote(
                        prod.at[zs, :, yt, :, cols_of(1, ct)], ret_x.at[self_at[1]],
                        ret_send.at[1], ret_recv.at[1], device(zs, x, yt, ct),
                    )
                else:
                    ret_y[self_at[0]] = prod[zs, x, :, :, cols_of(0, c)]
                    ret_x[self_at[1]] = prod[zs, :, y, :, cols_of(1, c)]
        for dx in range(4):
            for dy in range(4):
                for dc in range(2):
                    xt, yt, ct = wrap4(x + dx), wrap4(y + dy), c ^ dc
                    if dx or dy or dc:
                        remote(
                            prod.at[zs, xt, yt, :, cols_of(2, ct)], ret_z.at[self_at[2], zs],
                            ret_send.at[2], ret_recv.at[2], device(z, xt, yt, ct),
                        )
                    else:
                        ret_z[self_at[2], zs] = prod[zs, x, y, :, cols_of(2, c)]

    loads[8].wait()
    drain(att_in.at[:, pl.ds(0, 1792)], att_recv)

    def project(f, carry):
        at = pl.ds(aligned(f * 256, 256), 256)
        mo_ref[:, at] = dot(att_in[...], mix[:, at]).astype(BF16)
        return carry

    lax.fori_loop(0, 8, project, 0)

    for axis in AXES:
        drain(ag[axis].at[:, :, pl.ds(0, 112), :], ag_send.at[axis])
    for axis in (2, 1, 0):
        drain(ret[axis].at[pl.ds(0, 31)], ret_recv.at[axis])
        for step in (1, 3, 2, 0):
            j = wrap4(line_pos[axis] + step)
            rows = ret[axis][:, j].reshape(512, COLS[axis])
            part = dot(mixing[axis, j], rows).astype(BF16)
            ag[axis][j] = part.reshape(2, 128, COLS[axis])
            slot = (4 - step) % 4
            for dc in range(2):
                cc = c ^ dc
                if step or dc:
                    remote(
                        ag[axis].at[j, cc], rs[axis].at[c, slot],
                        rs_send.at[axis], rs_recv.at[axis], line_peer(axis, j, cc),
                    )
        rs[axis][c, 0] = ag[axis][line_pos[axis], c]
    for axis in (2, 1, 0):
        drain(rs[axis].at[:, :, pl.ds(0, 112), :], rs_recv.at[axis])
        for cc in range(2):
            parts = [rs[axis][cc, s].astype(F32) for s in range(4)]
            first = BASE[axis] + cc * COLS[axis]
            eo_ref[:, first : first + COLS[axis]] = (parts[0] + parts[1] + parts[2] + parts[3]).astype(BF16)

    drain(dummy, meta_send)
    drain(kx.at[pl.ds(0, 128)], halo_send.at[0])
    drain(kx.at[pl.ds(0, 128)], halo_send.at[1])
    drain(kx.at[pl.ds(0, 128)], halo_send.at[2])
    drain(kx.at[pl.ds(0, 128)], halo_send.at[3])
    drain(att_in.at[:, pl.ds(0, 1792)], att_send)
    for axis in AXES:
        drain(pk[axis].at[pl.ds(0, 31)], pk_send.at[axis])
        drain(ret[axis].at[pl.ds(0, 31)], ret_send.at[axis])
        drain(ag[axis].at[:, :, pl.ds(0, 112), :], rs_send.at[axis])


def body(
    queries, key_heads, value_heads, sink_logits, mix_weight, expert_input, norm_gain,
    routes, route_weights, gate_weight, up_weight, down_weight,
):
    row_cos, row_sin, col_cos, col_sin, pairs = rope_tables()
    meta = jnp.concatenate([routes.T.astype(F32), route_weights.T], axis=0)
    vmem = pl.BlockSpec(memory_space=pltpu.VMEM)
    hbm = pl.BlockSpec(memory_space=pl.ANY)
    dma = pltpu.SemaphoreType.DMA
    V = pltpu.VMEM
    scratch = [
        V((2048, 256), BF16), V((2304, 128), BF16), V((2304, 128), BF16),
        V((2304, 128), BF16), V((2304, 128), BF16), V((2304, 128), BF16),
        V((2048, 256), BF16), V((256, 2048), BF16),
        V((36, 1, 128), F32), V((36, 1, 128), F32),
        V((2048, 2048), BF16), V((2048, 1024), BF16), V((2048, 1024), BF16), V((1024, 2048), BF16),
        V((128, 2048), BF16), V((3, 4, 8, 256), F32),
        V((4, 2, 128, 512), BF16), V((4, 2, 128, 256), BF16), V((4, 2, 128, 256), BF16),
        V((32, 4, 16, 512), BF16), V((32, 4, 16, 256), BF16), V((32, 4, 16, 256), BF16),
        V((4, 4, 4, 16, 2048), BF16), V((256, 1024), BF16), V((4, 4, 4, 16, 2048), BF16),
        V((32, 4, 16, 512), BF16), V((32, 4, 16, 256), BF16), V((32, 4, 16, 256), BF16),
        V((3, 4, 256, 512), BF16),
        V((2, 4, 128, 512), BF16), V((2, 4, 128, 256), BF16), V((2, 4, 128, 256), BF16),
        V((8, 128), F32), V((168, 128), F32),
        dma((9,)), dma((4,)), dma((4,)), dma, dma, dma((3,)), dma((3,)),
        dma((3,)), dma((4,)), dma((4,)), dma, dma, dma, dma((3,)), dma((3,)), dma((3,)), dma((3,)),
    ]
    return pl.pallas_call(
        kernel,
        out_shape=(jax.ShapeDtypeStruct((256, 2048), BF16), jax.ShapeDtypeStruct((128, 2048), BF16)),
        in_specs=[pl.BlockSpec(memory_space=pltpu.SMEM)] + [vmem] * 6 + [hbm] * 9,
        out_specs=(vmem, vmem),
        scratch_shapes=scratch,
        compiler_params=pltpu.CompilerParams(
            collective_id=0, has_side_effects=True, vmem_limit_bytes=67043328
        ),
        name="layer",
    )(
        sink_logits, expert_input, norm_gain.reshape(1, -1), meta, jnp.asarray(pairs, BF16),
        jnp.asarray(col_cos), jnp.asarray(col_sin), jnp.asarray(row_cos), jnp.asarray(row_sin),
        queries, key_heads, value_heads, mix_weight, gate_weight, up_weight, down_weight,
    )


def solution(mesh):
    return jax.shard_map(
        body,
        mesh=mesh,
        in_specs=(
            P("ep", "tp"), P("ep", "tp"), P("ep", "tp"), P("tp"), P(), P(("ep", "tp"), None), P(),
            P(("ep", "tp"), None), P(("ep", "tp"), None), P(("ep", "tp"), None, None),
            P(("ep", "tp"), None, None), P(("ep", "tp"), None, None),
        ),
        out_specs=(P(("ep", "tp"), None), P(("ep", "tp"), None)),
        check_vma=False,
    )
```

time: 202 us -> 141 us (0.70)
  Pallas kernels: 0 us -> 134 us
  matrix products: 52 us -> 0 us
  waiting for transfers between devices: 45 us -> 0 us
  other arithmetic: 36.1 us -> 1.96 us
  starting transfers between devices: 32.8 us -> 0 us
  local copies, waits for them, and re-layouts: 31.1 us -> 4.18 us
  loops' own time: 2.87 us -> 0 us
    pallas_call x0 -> x1, Pallas kernels: none -> 134 us  [body(): pl.pallas_call(kernel, out_shape=(jax.ShapeDtypeStruct((256, 2048), BF16)...]
    dot_general x12 -> x0, matrix products: 52 us -> none  [the longest x4 15.6 us: one_block(): jnp.einsum('qkgd,skd->kgqs', q_blk, k_blk, preferred_element_type=jnp.flo...]
    all_to_all x3 -> x0, waiting for transfers between devices: 45 us -> none  [the longest x1 45 us: body(): lax.all_to_all(produced, ('ep', 'tp'), split_axis=0, concat_axis=0, tiled...]
    all_to_all x3 -> x0, starting transfers between devices: 27.6 us -> none  [the longest x1 12.6 us: body(): lax.all_to_all(outgoing, ('ep', 'tp'), split_axis=0, concat_axis=0, tiled...]
    reduce_sum x8 -> x0, other arithmetic: 24.2 us -> none  [the longest x4 17.1 us: one_block(): jnp.sum(weights_exp, axis=-1) + jnp.exp(sink_grid[:, :, None] - peak)]
    gather x3 -> x0, local copies, waits for them, and re-layouts: 15.3 us -> none  [the longest x2 9.35 us: body(): jnp.take(returned.reshape(experts * capacity, width), columns, axis=0)]
    ppermute x2 -> x0, starting transfers between devices: 5.22 us -> none  [the longest x1 3.92 us: with_halo(): lax.ppermute(tail, axis, [(i, (i + 1) % count) for i in range(ends)])]
    select_n x3 -> x0, other arithmetic: 4.66 us -> none  [the longest x1 4.65 us: body(): jnp.take(padded_in, table, axis=0).reshape(experts, capacity, width)]
  transfers between devices with their start and end apart: 5 -> 0, of which waited for: 1 -> 0; matrix products, arithmetic and copies ran while one was open for 49% -> 0% of each run, Pallas kernels for 0% -> 0%
where the time goes in v1:
time: 141 us; the launch traced here: 140 us
  Pallas kernels  134 us (95%)
  local copies, waits for them, and re-layouts  4.18 us (3%)
  other arithmetic  1.96 us (1%)
    pallas_call x1, Pallas kernels, body(): pl.pallas_call(kernel, out_shape=(jax.ShapeDtypeStruct((256, 2048), BF16)...  134 us
    unnamed x2, local copies, waits for them, and re-layouts  4.18 us

profile of v1, /device:TPU:1, one launch (start us, length us, event | category | flops | bytes accessed | tf_op | source)
XLA Modules:
  0.0 140.3 jit_solution(14983266862588686135)
XLA Ops:
  0.6 0.7 convert_bitcast_fusion
  1.3 1.3 pad_maximum_fusion.meta_ref
  2.6 133.5 %layer.1 = (bf16[256,2048]{1,0:T(8,128)(2,1)}, bf16[128,2048]{1,0:T(8,128)(2,1)}) custom-call(f32[4]{0:T(128)} %sink_ref.1, bf16[128,2048]{1,0:T(8,128)(2,1)} %x_ref.1, f32[1,2048]{1,0:T(1,128)} %bitcast.4, f32[8,128]{1,0:T(8,128)} %pad_maximum_fusion.meta_ref, bf16[256,256]{1,0:T(8,128)(2,1)} %constant.10.clone.pairs_ref, ...), custom_call_target="tpu_custom_call" | custom-call | tf_op jit(solution)/shard_map/layer/pallas_call | solution.py:466
  136.1 2.3 %copy.21 = bf16[256,2048]{1,0:T(8,128)(2,1)} copy(bf16[256,2048]{1,0:T(8,128)(2,1)} %get-tuple-element.4) | data formatting | bytes 2097152
  138.4 1.9 %copy.22 = bf16[128,2048]{1,0:T(8,128)(2,1)} copy(bf16[128,2048]{1,0:T(8,128)(2,1)} %get-tuple-element.5) | data formatting | bytes 1048576

commit v2 on v1

--- a/solution.py
+++ b/solution.py
@@ -1,5 +1,4 @@
-import functools
-import math
+import random
 
 import jax
 import jax.numpy as jnp
@@ -17,9 +16,26 @@
 CLAMP_LIMIT = 7.0
 GATE_SLOPE = 1.702
 NORM_EPS = 1e-05
-BASE = (0, 1024, 1536)
-COLS = (512, 256, 256)
+BASE = (0, 768, 1536)
+COLS = (384, 384, 256)
 AXES = (0, 1, 2)
+CHUNKS = ((1, 3), (2, 0))
+
+
+def shuffled(items):
+    return random.Random(1).sample(items, len(items))
+
+
+def messages(chunk, kinds):
+    pairs = [(a, b) for a in range(4) for b in range(2)]
+    items = []
+    for dz in CHUNKS[chunk]:
+        for axis in (0, 1):
+            if axis in kinds:
+                items += [(axis, dz, d, dc) for d, dc in pairs if dz or d or dc]
+        if 2 in kinds:
+            items += [(2, dz, dx, dy, dc) for dx in range(4) for dy, dc in pairs if dx or dy or dc]
+    return shuffled(items)
 
 
 def rope_tables():
@@ -61,14 +77,14 @@
 
 
 def kernel(
-    sink_ref, x_ref, gain_ref, meta_ref, pairs_ref, col_cos_ref, col_sin_ref,
+    sink_ref, x_ref, gain_ref, routes_ref, shares_ref, pairs_ref, col_cos_ref, col_sin_ref,
     row_cos_hbm, row_sin_hbm, q_hbm, k_hbm, v_hbm, mix_hbm, wg_hbm, wu_hbm, wd_hbm,
     mo_ref, eo_ref,
     q, kx, vx, krot, kswap, vswap, att, att_in, row_cos, row_sin, mix, wg, wu, wd,
     nrm, metas, ag_y, ag_x, ag_z, pk_y, pk_x, pk_z, arr, act, prod, ret_y, ret_x, ret_z,
     mixing, rs_y, rs_x, rs_z, own_meta, dummy,
     load_sem, halo_send, halo_recv, meta_send, meta_recv, ag_send, ag_recv,
-    pk_send, y_recv, x_recv, z_recv, att_send, att_recv, ret_send, ret_recv, rs_send, rs_recv,
+    pk_send, row_recv, att_send, att_recv, ret_send, ret_recv, rs_send, rs_recv,
 ):
     ep, tp = lax.axis_index("ep"), lax.axis_index("tp")
     z, x, y, c = ep // 4, lax.rem(ep, 4), tp // 2, lax.rem(tp, 2)
@@ -108,7 +124,7 @@
     spread = jnp.mean(jnp.square(moved), axis=-1, keepdims=True)
     nrm[...] = (moved * lax.rsqrt(spread + NORM_EPS) * gain_ref[...]).astype(BF16)
     expert_of = lax.broadcasted_iota(jnp.int32, (128, 128), 0).astype(F32)
-    routes = [meta_ref[k : k + 1, :] for k in range(4)]
+    routes = [routes_ref[k : k + 1, :].astype(F32) for k in range(4)]
     named = [(expert_of == routes[k]).astype(F32) for k in range(4)]
     named_any = named[0] + named[1] + named[2] + named[3]
     earlier = (
@@ -119,7 +135,7 @@
     for k in range(4):
         slot = jnp.sum(before * named[k], axis=0, keepdims=True)
         own_meta[k : k + 1, :] = routes[k] * 16.0 + core * 8.0 + slot
-    own_meta[4:8, :] = meta_ref[4:8, :]
+        own_meta[4 + k : 5 + k, :] = shares_ref[k : k + 1, :]
 
     pl.semaphore_wait(barrier, peers)
 
@@ -178,7 +194,6 @@
             return (e // 8) * 32 + x * 8 + lax.rem(e, 8)
         return z * 32 + e
 
-    drain(dummy, meta_recv)
     self_at = ((z * 4 + x) * 2 + c, (z * 4 + y) * 2 + c, (x * 4 + y) * 2 + c)
 
     def pack(axis):
@@ -200,40 +215,22 @@
     def cols_of(axis, cc):
         return pl.ds(aligned(BASE[axis] + cc * COLS[axis]), COLS[axis])
 
-    pack(2)
-    for dx, dy, dc in [(a, b, d) for a in range(4) for b in range(4) for d in range(2)]:
-        xt, yt, ct = wrap4(x + dx), wrap4(y + dy), c ^ dc
-        if dx or dy or dc:
-            remote(
-                pk_z.at[(xt * 4 + yt) * 2 + ct], arr.at[:, x, y, :, cols_of(2, c)],
-                pk_send.at[2], z_recv, device(z, xt, yt, ct),
-            )
-    arr[:, x, y, :, cols_of(2, c)] = pk_z[self_at[2]]
-    pack(1)
-    for dz, dy, dc in [(a, b, d) for a in range(4) for b in range(4) for d in range(2)]:
-        zt, yt, ct = wrap4(z + dz), wrap4(y + dy), c ^ dc
-        if dz or dy or dc:
-            remote(
-                pk_x.at[(zt * 4 + yt) * 2 + ct], arr.at[z, :, y, :, cols_of(1, c)],
-                pk_send.at[1], x_recv.at[dz], device(zt, x, yt, ct),
-            )
-    arr[z, :, y, :, cols_of(1, c)] = pk_x[self_at[1]]
-    pack(0)
-    for dz, dx, dc in [(a, b, d) for a in range(4) for b in range(4) for d in range(2)]:
-        zt, xt, ct = wrap4(z + dz), wrap4(x + dx), c ^ dc
-        if dz or dx or dc:
-            remote(
-                pk_y.at[(zt * 4 + xt) * 2 + ct], arr.at[z, x, :, :, cols_of(0, c)],
-                pk_send.at[0], y_recv.at[dz], device(zt, xt, y, ct),
-            )
-    arr[z, x, :, :, cols_of(0, c)] = pk_y[self_at[0]]
+    def weigh_axis(axis):
+        r = lax.broadcasted_iota(jnp.int32, (256, 512), 1)
+        key = (plane_expert(axis, r // 16) * 16 + lax.rem(r, 16)).astype(F32)
+
+        def weigh(j, carry):
+            turned = jnp.transpose(metas[axis, j])
+            share = jnp.zeros((256, 512), F32)
+            for k in range(4):
+                share += jnp.where(key == turned[:, k : k + 1], turned[:, 4 + k : 5 + k], 0.0)
+            mixing[axis, j] = share.astype(BF16)
+            return carry
+
+        lax.fori_loop(0, 4, weigh, 0)
 
     for copy in loads[:5]:
         copy.wait()
-    drain(kx.at[pl.ds(0, 128)], halo_recv.at[0])
-    drain(kx.at[pl.ds(2176, 128)], halo_recv.at[1])
-    drain(vx.at[pl.ds(0, 128)], halo_recv.at[2])
-    drain(vx.at[pl.ds(2176, 128)], halo_recv.at[3])
     low = lax.rem(lax.broadcasted_iota(jnp.int32, (128, 128), 1), 128) < 64
 
     def turn_tables(g):
@@ -251,7 +248,7 @@
         vswap[at, :] = pltpu.roll(vx[at, :].astype(F32), 64, 1).astype(BF16)
         return carry
 
-    lax.fori_loop(0, 18, turn_keys, 0)
+    lax.fori_loop(1, 17, turn_keys, 0)
     i_at = lax.broadcasted_iota(jnp.int32, (256, 128), 0)
     i_at = lax.rem(i_at, 128)
     j_at = lax.broadcasted_iota(jnp.int32, (256, 128), 1)
@@ -314,39 +311,59 @@
 
         return carry
 
-    lax.fori_loop(0, 8, attend_for, 0)
+    drain(dummy, meta_recv)
+    weigh_axis(2)
+    weigh_axis(1)
+    def send_rows(items):
+        for axis, dz, *rest in items:
+            if axis == 0:
+                zt, xt, ct = wrap4(z + dz), wrap4(x + rest[0]), c ^ rest[1]
+                src, dst = pk_y.at[(zt * 4 + xt) * 2 + ct], arr.at[z, x, :, :, cols_of(0, c)]
+                target = device(zt, xt, y, ct)
+            elif axis == 1:
+                zt, yt, ct = wrap4(z + dz), wrap4(y + rest[0]), c ^ rest[1]
+                src, dst = pk_x.at[(zt * 4 + yt) * 2 + ct], arr.at[z, :, y, :, cols_of(1, c)]
+                target = device(zt, x, yt, ct)
+            else:
+                xt, yt, ct = wrap4(x + rest[0]), wrap4(y + rest[1]), c ^ rest[2]
+                zs = wrap4(z + 4 - dz)
+                src, dst = pk_z.at[(xt * 4 + yt) * 2 + ct, zs], arr.at[zs, x, y, :, cols_of(2, c)]
+                target = device(z, xt, yt, ct)
+            chunk = 0 if dz in CHUNKS[0] else 1
+            remote(src, dst, pk_send.at[axis], row_recv.at[axis, chunk], target)
+
+    pack(2)
+    send_rows(messages(0, (2,)))
+    pack(1)
+    pack(0)
+    send_rows(messages(0, (0, 1)))
+    arr[:, x, y, :, cols_of(2, c)] = pk_z[self_at[2]]
+    arr[z, :, y, :, cols_of(1, c)] = pk_x[self_at[1]]
+    arr[z, x, :, :, cols_of(0, c)] = pk_y[self_at[0]]
+
+    drain(kx.at[pl.ds(0, 128)], halo_recv.at[0])
+    drain(kx.at[pl.ds(2176, 128)], halo_recv.at[1])
+    drain(vx.at[pl.ds(0, 128)], halo_recv.at[2])
+    drain(vx.at[pl.ds(2176, 128)], halo_recv.at[3])
+    turn_keys(0, 0)
+    turn_keys(17, 0)
+    lax.fori_loop(0, 3, attend_for, 0)
+    send_rows(messages(1, (0, 1, 2)))
+    lax.fori_loop(3, 8, attend_for, 0)
+    weigh_axis(0)
     att_in[:, pl.ds(aligned(tp * 256), 256)] = att[pl.ds(aligned(tp * 256, 256), 256), :]
-
-    for axis in AXES:
-        r = lax.broadcasted_iota(jnp.int32, (256, 512), 1)
-        key = (plane_expert(axis, r // 16) * 16 + lax.rem(r, 16)).astype(F32)
-
-        def weigh(j, carry):
-            turned = jnp.transpose(metas[axis, j])
-            share = jnp.zeros((256, 512), F32)
-            for k in range(4):
-                share += jnp.where(key == turned[:, k : k + 1], turned[:, 4 + k : 5 + k], 0.0)
-            mixing[axis, j] = share.astype(BF16)
-            return carry
-
-        lax.fori_loop(0, 4, weigh, 0)
 
     for copy in loads[5:8]:
         copy.wait()
-    drain(pk_z.at[pl.ds(0, 31)], z_recv)
-
-    for dz in range(4):
-        zs = wrap4(z + 4 - dz)
-        if dz == 0:
-            drain(arr.at[0, :, :, :, pl.ds(0, 896)], y_recv.at[0])
-            drain(arr.at[0, pl.ds(0, 2), :, :, pl.ds(0, 896)], x_recv.at[0])
-        else:
-            drain(arr.at[0, :, :, :, pl.ds(0, 1024)], y_recv.at[dz])
-            drain(arr.at[0, :, :, :, pl.ds(0, 512)], x_recv.at[dz])
+    for chunk in range(2):
+        drain(pk_y.at[pl.ds(0, 16 - chunk)], row_recv.at[0, chunk])
+        drain(pk_x.at[pl.ds(0, 16 - chunk)], row_recv.at[1, chunk])
+        drain(pk_z.at[pl.ds(0, 31), pl.ds(0, 2)], row_recv.at[2, chunk])
+        z0, z1 = [wrap4(z + 4 - dz) for dz in CHUNKS[chunk]]
 
         def hidden(f, carry):
             at = pl.ds(aligned(f * 256, 256), 256)
-            rows = arr[zs].reshape(256, 2048)
+            rows = jnp.concatenate([arr[z0].reshape(256, 2048), arr[z1].reshape(256, 2048)], axis=0)
             gate = jnp.minimum(dot(rows, wg[:, at]), CLAMP_LIMIT)
             lift = jnp.clip(dot(rows, wu[:, at]), -CLAMP_LIMIT, CLAMP_LIMIT)
             act[:, at] = ((lift + 1.0) * gate * jax.nn.sigmoid(GATE_SLOPE * gate)).astype(BF16)
@@ -357,37 +374,32 @@
         def down(f, carry):
             at = pl.ds(aligned(f * 256, 256), 256)
             res = dot(act[...], wd[:, at]).astype(BF16)
-            prod[zs, :, :, :, at] = res.reshape(4, 4, 16, 256)
+            prod[z0, :, :, :, at] = res[:256].reshape(4, 4, 16, 256)
+            prod[z1, :, :, :, at] = res[256:].reshape(4, 4, 16, 256)
             return carry
 
         lax.fori_loop(0, 8, down, 0)
 
-        for d1 in range(4):
-            for dc in range(2):
-                xt, yt, ct = wrap4(x + d1), wrap4(y + d1), c ^ dc
-                if dz or d1 or dc:
-                    remote(
-                        prod.at[zs, xt, :, :, cols_of(0, ct)], ret_y.at[self_at[0]],
-                        ret_send.at[0], ret_recv.at[0], device(zs, xt, y, ct),
-                    )
-                    remote(
-                        prod.at[zs, :, yt, :, cols_of(1, ct)], ret_x.at[self_at[1]],
-                        ret_send.at[1], ret_recv.at[1], device(zs, x, yt, ct),
-                    )
-                else:
-                    ret_y[self_at[0]] = prod[zs, x, :, :, cols_of(0, c)]
-                    ret_x[self_at[1]] = prod[zs, :, y, :, cols_of(1, c)]
-        for dx in range(4):
-            for dy in range(4):
-                for dc in range(2):
-                    xt, yt, ct = wrap4(x + dx), wrap4(y + dy), c ^ dc
-                    if dx or dy or dc:
-                        remote(
-                            prod.at[zs, xt, yt, :, cols_of(2, ct)], ret_z.at[self_at[2], zs],
-                            ret_send.at[2], ret_recv.at[2], device(z, xt, yt, ct),
-                        )
-                    else:
-                        ret_z[self_at[2], zs] = prod[zs, x, y, :, cols_of(2, c)]
+        for axis, dz, *rest in messages(chunk, (0, 1, 2)):
+            zs = wrap4(z + 4 - dz)
+            if axis == 0:
+                xt, ct = wrap4(x + rest[0]), c ^ rest[1]
+                src, dst = prod.at[zs, xt, :, :, cols_of(0, ct)], ret_y.at[self_at[0]]
+                target = device(zs, xt, y, ct)
+            elif axis == 1:
+                yt, ct = wrap4(y + rest[0]), c ^ rest[1]
+                src, dst = prod.at[zs, :, yt, :, cols_of(1, ct)], ret_x.at[self_at[1]]
+                target = device(zs, x, yt, ct)
+            else:
+                xt, yt, ct = wrap4(x + rest[0]), wrap4(y + rest[1]), c ^ rest[2]
+                src, dst = prod.at[zs, xt, yt, :, cols_of(2, ct)], ret_z.at[self_at[2], zs]
+                target = device(z, xt, yt, ct)
+            remote(src, dst, ret_send.at[axis], ret_recv.at[axis], target)
+        if chunk == 1:
+            ret_y[self_at[0]] = prod[z, x, :, :, cols_of(0, c)]
+            ret_x[self_at[1]] = prod[z, :, y, :, cols_of(1, c)]
+        for zs in (z0, z1):
+            ret_z[self_at[2], zs] = prod[zs, x, y, :, cols_of(2, c)]
 
     loads[8].wait()
     drain(att_in.at[:, pl.ds(0, 1792)], att_recv)
@@ -441,7 +453,6 @@
     routes, route_weights, gate_weight, up_weight, down_weight,
 ):
     row_cos, row_sin, col_cos, col_sin, pairs = rope_tables()
-    meta = jnp.concatenate([routes.T.astype(F32), route_weights.T], axis=0)
     vmem = pl.BlockSpec(memory_space=pltpu.VMEM)
     hbm = pl.BlockSpec(memory_space=pl.ANY)
     dma = pltpu.SemaphoreType.DMA
@@ -453,20 +464,20 @@
         V((36, 1, 128), F32), V((36, 1, 128), F32),
         V((2048, 2048), BF16), V((2048, 1024), BF16), V((2048, 1024), BF16), V((1024, 2048), BF16),
         V((128, 2048), BF16), V((3, 4, 8, 256), F32),
-        V((4, 2, 128, 512), BF16), V((4, 2, 128, 256), BF16), V((4, 2, 128, 256), BF16),
-        V((32, 4, 16, 512), BF16), V((32, 4, 16, 256), BF16), V((32, 4, 16, 256), BF16),
-        V((4, 4, 4, 16, 2048), BF16), V((256, 1024), BF16), V((4, 4, 4, 16, 2048), BF16),
-        V((32, 4, 16, 512), BF16), V((32, 4, 16, 256), BF16), V((32, 4, 16, 256), BF16),
+        *[V((4, 2, 128, n), BF16) for n in COLS],
+        *[V((32, 4, 16, n), BF16) for n in COLS],
+        V((4, 4, 4, 16, 2048), BF16), V((512, 1024), BF16), V((4, 4, 4, 16, 2048), BF16),
+        *[V((32, 4, 16, n), BF16) for n in COLS],
         V((3, 4, 256, 512), BF16),
-        V((2, 4, 128, 512), BF16), V((2, 4, 128, 256), BF16), V((2, 4, 128, 256), BF16),
+        *[V((2, 4, 128, n), BF16) for n in COLS],
         V((8, 128), F32), V((168, 128), F32),
         dma((9,)), dma((4,)), dma((4,)), dma, dma, dma((3,)), dma((3,)),
-        dma((3,)), dma((4,)), dma((4,)), dma, dma, dma, dma((3,)), dma((3,)), dma((3,)), dma((3,)),
+        dma((3,)), dma((3, 2)), dma, dma, dma((3,)), dma((3,)), dma((3,)), dma((3,)),
     ]
-    return pl.pallas_call(
+    mixed, summed = pl.pallas_call(
         kernel,
         out_shape=(jax.ShapeDtypeStruct((256, 2048), BF16), jax.ShapeDtypeStruct((128, 2048), BF16)),
-        in_specs=[pl.BlockSpec(memory_space=pltpu.SMEM)] + [vmem] * 6 + [hbm] * 9,
+        in_specs=[pl.BlockSpec(memory_space=pltpu.SMEM)] + [vmem] * 7 + [hbm] * 9,
         out_specs=(vmem, vmem),
         scratch_shapes=scratch,
         compiler_params=pltpu.CompilerParams(
@@ -474,10 +485,34 @@
         ),
         name="layer",
     )(
-        sink_logits, expert_input, norm_gain.reshape(1, -1), meta, jnp.asarray(pairs, BF16),
+        sink_logits, expert_input, norm_gain.reshape(1, -1), routes.T, route_weights.T, jnp.asarray(pairs, BF16),
         jnp.asarray(col_cos), jnp.asarray(col_sin), jnp.asarray(row_cos), jnp.asarray(row_sin),
         queries, key_heads, value_heads, mix_weight, gate_weight, up_weight, down_weight,
     )
+    return pl.pallas_call(
+        hand_over,
+        out_shape=(jax.ShapeDtypeStruct((256, 2048), BF16), jax.ShapeDtypeStruct((128, 2048), BF16)),
+        in_specs=[hbm] * 2,
+        out_specs=(hbm, hbm),
+        scratch_shapes=[V((384, 2048), BF16), dma((3,)), dma((3,))],
+        name="finish",
+    )(mixed, summed)
+
+
+def hand_over(mixed, summed, mixed_out, summed_out, held, in_sem, out_sem):
+    parts = [(mixed, mixed_out, 0, 0), (mixed, mixed_out, 128, 128), (summed, summed_out, 0, 256)]
+    takes, gives = [], []
+    for n, (src, dst, first, at) in enumerate(parts):
+        here = held.at[pl.ds(at, 128)]
+        takes.append(pltpu.make_async_copy(src.at[pl.ds(first, 128)], here, in_sem.at[n]))
+        gives.append(pltpu.make_async_copy(here, dst.at[pl.ds(first, 128)], out_sem.at[n]))
+    for copy in takes:
+        copy.start()
+    for take, give in zip(takes, gives):
+        take.wait()
+        give.start()
+    for copy in gives:
+        copy.wait()
 
 
 def solution(mesh):

time: 141 us -> 119 us (0.84); the launches traced: 140 us -> 117 us
  Pallas kernels: 134 us -> 116 us
  local copies, waits for them, and re-layouts: 4.18 us -> 0 us
  other arithmetic: 1.96 us -> 0 us
    pallas_call x1, Pallas kernels: 134 us -> 114 us  [body(): pl.pallas_call(kernel, out_shape=(jax.ShapeDtypeStruct((256, 2048), BF16)...]
    unnamed x2 -> x0, local copies, waits for them, and re-layouts: 4.18 us -> none
    pallas_call x0 -> x1, Pallas kernels: none -> 2.23 us  [body(): pl.pallas_call(hand_over, out_shape=(jax.ShapeDtypeStruct((256, 2048), BF...]
where the time goes in v2:
time: 119 us; the launch traced here: 117 us
  Pallas kernels  116 us (97%)
    pallas_call x1, Pallas kernels, body(): pl.pallas_call(kernel, out_shape=(jax.ShapeDtypeStruct((256, 2048), BF16)...  114 us

profile of v2, /device:TPU:1, one launch (start us, length us, event | category | flops | bytes accessed | tf_op | source)
XLA Modules:
  0.0 116.8 jit_solution(14468717868401458756)
XLA Ops:
  0.6 113.9 %layer.1 = (bf16[256,2048]{1,0:T(8,128)(2,1)}, bf16[128,2048]{1,0:T(8,128)(2,1)}) custom-call(f32[4]{0:T(128)} %sink_ref.1, bf16[128,2048]{1,0:T(8,128)(2,1)} %x_ref.1, f32[1,2048]{1,0:T(1,128)} %bitcast.3, s32[4,128]{1,0:T(4,128)} %bitcast.4, f32[4,128]{1,0:T(4,128)} %bitcast.5, bf16[256,256]{1,0:T(8,128)(2,1)} %constant.10.clone.pairs_ref, ...), custom_call_target="tpu_custom_call" | custom-call | tf_op jit(solution)/shard_map/layer/pallas_call | solution.py:477
  114.6 2.2 %finish.1 = (bf16[256,2048]{1,0:T(8,128)(2,1)}, bf16[128,2048]{1,0:T(8,128)(2,1)}) custom-call(bf16[256,2048]{1,0:T(8,128)(2,1)} %get-tuple-element.4.mixed, bf16[128,2048]{1,0:T(8,128)(2,1)} %get-tuple-element.5.summed), custom_call_target="tpu_custom_call" | custom-call | tf_op jit(solution)/shard_map/finish/pallas_call | solution.py:492

commit v3 on v2

--- a/solution.py
+++ b/solution.py
@@ -18,6 +18,8 @@
 NORM_EPS = 1e-05
 BASE = (0, 768, 1536)
 COLS = (384, 384, 256)
+BACK_BASE = (0, 768, 1536)
+BACK_COLS = (384, 384, 256)
 AXES = (0, 1, 2)
 CHUNKS = ((1, 3), (2, 0))
 
@@ -32,7 +34,7 @@
     for dz in CHUNKS[chunk]:
         for axis in (0, 1):
             if axis in kinds:
-                items += [(axis, dz, d, dc) for d, dc in pairs if dz or d or dc]
+                items += [(axis, dz, d, dc, n) for d, dc in pairs if dz or d or dc for n in range(4)]
         if 2 in kinds:
             items += [(2, dz, dx, dy, dc) for dx in range(4) for dy, dc in pairs if dx or dy or dc]
     return shuffled(items)
@@ -77,18 +79,19 @@
 
 
 def kernel(
-    sink_ref, x_ref, gain_ref, routes_ref, shares_ref, pairs_ref, col_cos_ref, col_sin_ref,
+    sink_ref, x_hbm, gain_hbm, routes_hbm, shares_hbm, pairs_hbm, col_cos_hbm, col_sin_hbm,
     row_cos_hbm, row_sin_hbm, q_hbm, k_hbm, v_hbm, mix_hbm, wg_hbm, wu_hbm, wd_hbm,
-    mo_ref, eo_ref,
-    q, kx, vx, krot, kswap, vswap, att, att_in, row_cos, row_sin, mix, wg, wu, wd,
+    mo_hbm, eo_hbm,
+    x_ref, gain_ref, routes_ref, shares_ref, pairs_ref, col_cos_ref, col_sin_ref, mo_ref, eo_ref, give_sem, q, kx, vx, krot, kswap, vswap, att, att_in, row_cos, row_sin, mix, wg, wu, wd,
     nrm, metas, ag_y, ag_x, ag_z, pk_y, pk_x, pk_z, arr, act, prod, ret_y, ret_x, ret_z,
-    mixing, rs_y, rs_x, rs_z, own_meta, dummy,
+    mixing, picks, rs_y, rs_x, rs_z, out_y, out_x, out_z, own_meta, dummy,
     load_sem, halo_send, halo_recv, meta_send, meta_recv, ag_send, ag_recv,
     pk_send, row_recv, att_send, att_recv, ret_send, ret_recv, rs_send, rs_recv,
 ):
     ep, tp = lax.axis_index("ep"), lax.axis_index("tp")
     z, x, y, c = ep // 4, lax.rem(ep, 4), tp // 2, lax.rem(tp, 2)
     ag, pk, ret, rs = (ag_y, ag_x, ag_z), (pk_y, pk_x, pk_z), (ret_y, ret_x, ret_z), (rs_y, rs_x, rs_z)
+    out = (out_y, out_x, out_z)
 
     barrier = pltpu.get_barrier_semaphore()
     peers = 0
@@ -115,8 +118,19 @@
         pltpu.make_async_copy(wd_hbm.at[0], wd, load_sem.at[7]),
         pltpu.make_async_copy(mix_hbm, mix, load_sem.at[8]),
     ]
-    for copy in loads:
+    first_loads = [
+        pltpu.make_async_copy(src, dst, load_sem.at[9 + n])
+        for n, (src, dst) in enumerate(
+            (
+                (x_hbm, x_ref), (gain_hbm, gain_ref), (routes_hbm, routes_ref), (shares_hbm, shares_ref),
+                (pairs_hbm, pairs_ref), (col_cos_hbm, col_cos_ref), (col_sin_hbm, col_sin_ref),
+            )
+        )
+    ]
+    for copy in first_loads + loads:
         copy.start()
+    for copy in first_loads:
+        copy.wait()
 
     values = x_ref[...].astype(F32)
     center = jnp.mean(values, axis=-1, keepdims=True)
@@ -156,7 +170,7 @@
     def drain(ref, sem):
         pltpu.make_async_copy(ref, ref, sem).wait()
 
-    line_steps = [(0, 1), (1, 0), (1, 1), (3, 0), (3, 1), (2, 0), (2, 1)]
+    line_steps = [(2, 0), (2, 1), (1, 0), (3, 0), (1, 1), (3, 1), (0, 1)]
     for axis in AXES:
         for step, dc in line_steps:
             j = wrap4(line_pos[axis] + step)
@@ -196,8 +210,7 @@
 
     self_at = ((z * 4 + x) * 2 + c, (z * 4 + y) * 2 + c, (x * 4 + y) * 2 + c)
 
-    def pack(axis):
-        drain(ag[axis].at[:, :, pl.ds(0, 112), :], ag_recv.at[axis])
+    def place(axis):
         r = lax.broadcasted_iota(jnp.int32, (512, 256), 0)
         key = (plane_expert(axis, r // 16) * 16 + lax.rem(r, 16)).astype(F32)
 
@@ -205,15 +218,22 @@
             hit = key == metas[axis, j, 0:1, :]
             for k in range(1, 4):
                 hit = hit | (key == metas[axis, j, k : k + 1, :])
-            rows = ag[axis][j].reshape(256, COLS[axis])
-            packed = dot(hit.astype(F32).astype(BF16), rows).astype(BF16)
+            picks[axis, j] = hit.astype(F32).astype(BF16)
+            return carry
+
+        lax.fori_loop(0, 4, one, 0)
+
+    def pack(axis):
+        drain(ag[axis].at[:, :, pl.ds(0, 112), :], ag_recv.at[axis])
+        for j in range(4):
+            packed = dot(picks[axis, j], ag[axis][j].reshape(256, COLS[axis])).astype(BF16)
             pk[axis][:, j] = packed.reshape(32, 16, COLS[axis])
-            return carry
-
-        lax.fori_loop(0, 4, one, 0)
 
     def cols_of(axis, cc):
         return pl.ds(aligned(BASE[axis] + cc * COLS[axis]), COLS[axis])
+
+    def back_cols(axis, cc):
+        return pl.ds(aligned(BACK_BASE[axis] + cc * BACK_COLS[axis]), BACK_COLS[axis])
 
     def weigh_axis(axis):
         r = lax.broadcasted_iota(jnp.int32, (256, 512), 1)
@@ -312,31 +332,32 @@
         return carry
 
     drain(dummy, meta_recv)
-    weigh_axis(2)
-    weigh_axis(1)
+    place(2)
+    place(1)
+    place(0)
     def send_rows(items):
         for axis, dz, *rest in items:
             if axis == 0:
                 zt, xt, ct = wrap4(z + dz), wrap4(x + rest[0]), c ^ rest[1]
-                src, dst = pk_y.at[(zt * 4 + xt) * 2 + ct], arr.at[z, x, :, :, cols_of(0, c)]
+                src, dst = pk_y.at[(zt * 4 + xt) * 2 + ct, rest[2]], arr.at[z, x, rest[2], :, cols_of(0, c)]
                 target = device(zt, xt, y, ct)
             elif axis == 1:
                 zt, yt, ct = wrap4(z + dz), wrap4(y + rest[0]), c ^ rest[1]
-                src, dst = pk_x.at[(zt * 4 + yt) * 2 + ct], arr.at[z, :, y, :, cols_of(1, c)]
+                src, dst = pk_x.at[(zt * 4 + yt) * 2 + ct, rest[2]], arr.at[z, rest[2], y, :, cols_of(1, c)]
                 target = device(zt, x, yt, ct)
             else:
                 xt, yt, ct = wrap4(x + rest[0]), wrap4(y + rest[1]), c ^ rest[2]
                 zs = wrap4(z + 4 - dz)
                 src, dst = pk_z.at[(xt * 4 + yt) * 2 + ct, zs], arr.at[zs, x, y, :, cols_of(2, c)]
                 target = device(z, xt, yt, ct)
-            chunk = 0 if dz in CHUNKS[0] else 1
+            chunk = [n for n, steps in enumerate(CHUNKS) if dz in steps][0]
             remote(src, dst, pk_send.at[axis], row_recv.at[axis, chunk], target)
 
     pack(2)
-    send_rows(messages(0, (2,)))
     pack(1)
+    send_rows(messages(0, (1, 2)))
     pack(0)
-    send_rows(messages(0, (0, 1)))
+    send_rows(messages(0, (0,)))
     arr[:, x, y, :, cols_of(2, c)] = pk_z[self_at[2]]
     arr[z, :, y, :, cols_of(1, c)] = pk_x[self_at[1]]
     arr[z, x, :, :, cols_of(0, c)] = pk_y[self_at[0]]
@@ -347,59 +368,64 @@
     drain(vx.at[pl.ds(2176, 128)], halo_recv.at[3])
     turn_keys(0, 0)
     turn_keys(17, 0)
-    lax.fori_loop(0, 3, attend_for, 0)
+    lax.fori_loop(0, 4, attend_for, 0)
     send_rows(messages(1, (0, 1, 2)))
-    lax.fori_loop(3, 8, attend_for, 0)
-    weigh_axis(0)
-    att_in[:, pl.ds(aligned(tp * 256), 256)] = att[pl.ds(aligned(tp * 256, 256), 256), :]
+    lax.fori_loop(4, 8, attend_for, 0)
 
     for copy in loads[5:8]:
         copy.wait()
-    for chunk in range(2):
-        drain(pk_y.at[pl.ds(0, 16 - chunk)], row_recv.at[0, chunk])
-        drain(pk_x.at[pl.ds(0, 16 - chunk)], row_recv.at[1, chunk])
-        drain(pk_z.at[pl.ds(0, 31), pl.ds(0, 2)], row_recv.at[2, chunk])
-        z0, z1 = [wrap4(z + 4 - dz) for dz in CHUNKS[chunk]]
+    for chunk, steps in enumerate(CHUNKS):
+        count = 8 * len(steps) - (0 in steps)
+        drain(pk_y.at[pl.ds(0, count)], row_recv.at[0, chunk])
+        drain(pk_x.at[pl.ds(0, count)], row_recv.at[1, chunk])
+        drain(pk_z.at[pl.ds(0, 31), pl.ds(0, len(steps))], row_recv.at[2, chunk])
+        sources = [wrap4(z + 4 - dz) for dz in steps]
+        here = pl.ds(0, 256 * len(steps))
 
         def hidden(f, carry):
             at = pl.ds(aligned(f * 256, 256), 256)
-            rows = jnp.concatenate([arr[z0].reshape(256, 2048), arr[z1].reshape(256, 2048)], axis=0)
+            rows = jnp.concatenate([arr[zs].reshape(256, 2048) for zs in sources], axis=0)
             gate = jnp.minimum(dot(rows, wg[:, at]), CLAMP_LIMIT)
             lift = jnp.clip(dot(rows, wu[:, at]), -CLAMP_LIMIT, CLAMP_LIMIT)
-            act[:, at] = ((lift + 1.0) * gate * jax.nn.sigmoid(GATE_SLOPE * gate)).astype(BF16)
+            act[here, at] = ((lift + 1.0) * gate * jax.nn.sigmoid(GATE_SLOPE * gate)).astype(BF16)
             return carry
 
         lax.fori_loop(0, 4, hidden, 0)
 
         def down(f, carry):
             at = pl.ds(aligned(f * 256, 256), 256)
-            res = dot(act[...], wd[:, at]).astype(BF16)
-            prod[z0, :, :, :, at] = res[:256].reshape(4, 4, 16, 256)
-            prod[z1, :, :, :, at] = res[256:].reshape(4, 4, 16, 256)
+            res = dot(act[here, :], wd[:, at]).astype(BF16)
+            for n, zs in enumerate(sources):
+                prod[zs, :, :, :, at] = res[256 * n : 256 * n + 256].reshape(4, 4, 16, 256)
             return carry
 
-        lax.fori_loop(0, 8, down, 0)
-
-        for axis, dz, *rest in messages(chunk, (0, 1, 2)):
-            zs = wrap4(z + 4 - dz)
-            if axis == 0:
-                xt, ct = wrap4(x + rest[0]), c ^ rest[1]
-                src, dst = prod.at[zs, xt, :, :, cols_of(0, ct)], ret_y.at[self_at[0]]
-                target = device(zs, xt, y, ct)
-            elif axis == 1:
-                yt, ct = wrap4(y + rest[0]), c ^ rest[1]
-                src, dst = prod.at[zs, :, yt, :, cols_of(1, ct)], ret_x.at[self_at[1]]
-                target = device(zs, x, yt, ct)
-            else:
-                xt, yt, ct = wrap4(x + rest[0]), wrap4(y + rest[1]), c ^ rest[2]
-                src, dst = prod.at[zs, xt, yt, :, cols_of(2, ct)], ret_z.at[self_at[2], zs]
-                target = device(z, xt, yt, ct)
-            remote(src, dst, ret_send.at[axis], ret_recv.at[axis], target)
-        if chunk == 1:
-            ret_y[self_at[0]] = prod[z, x, :, :, cols_of(0, c)]
-            ret_x[self_at[1]] = prod[z, :, y, :, cols_of(1, c)]
-        for zs in (z0, z1):
-            ret_z[self_at[2], zs] = prod[zs, x, y, :, cols_of(2, c)]
+        for kind in AXES:
+            first = BACK_BASE[kind] // 256
+            lax.fori_loop(first, first + BACK_COLS[kind] // 128, down, 0)
+            for axis, dz, *rest in messages(chunk, (kind,)):
+                zs = wrap4(z + 4 - dz)
+                if axis == 0:
+                    xt, ct = wrap4(x + rest[0]), c ^ rest[1]
+                    src, dst = prod.at[zs, xt, rest[2], :, back_cols(0, ct)], ret_y.at[self_at[0], rest[2]]
+                    target = device(zs, xt, y, ct)
+                elif axis == 1:
+                    yt, ct = wrap4(y + rest[0]), c ^ rest[1]
+                    src, dst = prod.at[zs, rest[2], yt, :, back_cols(1, ct)], ret_x.at[self_at[1], rest[2]]
+                    target = device(zs, x, yt, ct)
+                else:
+                    xt, yt, ct = wrap4(x + rest[0]), wrap4(y + rest[1]), c ^ rest[2]
+                    src, dst = prod.at[zs, xt, yt, :, back_cols(2, ct)], ret_z.at[self_at[2], zs]
+                    target = device(z, xt, yt, ct)
+                remote(src, dst, ret_send.at[axis], ret_recv.at[axis], target)
+        if 0 in steps:
+            ret_y[self_at[0]] = prod[z, x, :, :, back_cols(0, c)]
+            ret_x[self_at[1]] = prod[z, :, y, :, back_cols(1, c)]
+        for zs in sources:
+            ret_z[self_at[2], zs] = prod[zs, x, y, :, back_cols(2, c)]
+
+    att_in[:, pl.ds(aligned(tp * 256), 256)] = att[pl.ds(aligned(tp * 256, 256), 256), :]
+    for axis in AXES:
+        weigh_axis(axis)
 
     loads[8].wait()
     drain(att_in.at[:, pl.ds(0, 1792)], att_recv)
@@ -410,32 +436,34 @@
         return carry
 
     lax.fori_loop(0, 8, project, 0)
-
-    for axis in AXES:
-        drain(ag[axis].at[:, :, pl.ds(0, 112), :], ag_send.at[axis])
-    for axis in (2, 1, 0):
+    give_mixed = pltpu.make_async_copy(mo_ref, mo_hbm, give_sem.at[0])
+    give_mixed.start()
+
+    for axis in (0, 1, 2):
         drain(ret[axis].at[pl.ds(0, 31)], ret_recv.at[axis])
-        for step in (1, 3, 2, 0):
+        for step in (2, 1, 3, 0):
             j = wrap4(line_pos[axis] + step)
-            rows = ret[axis][:, j].reshape(512, COLS[axis])
+            rows = ret[axis][:, j].reshape(512, BACK_COLS[axis])
             part = dot(mixing[axis, j], rows).astype(BF16)
-            ag[axis][j] = part.reshape(2, 128, COLS[axis])
+            out[axis][j] = part.reshape(2, 128, BACK_COLS[axis])
             slot = (4 - step) % 4
             for dc in range(2):
                 cc = c ^ dc
                 if step or dc:
                     remote(
-                        ag[axis].at[j, cc], rs[axis].at[c, slot],
+                        out[axis].at[j, cc], rs[axis].at[c, slot],
                         rs_send.at[axis], rs_recv.at[axis], line_peer(axis, j, cc),
                     )
-        rs[axis][c, 0] = ag[axis][line_pos[axis], c]
-    for axis in (2, 1, 0):
+        rs[axis][c, 0] = out[axis][line_pos[axis], c]
+    for axis in (0, 1, 2):
         drain(rs[axis].at[:, :, pl.ds(0, 112), :], rs_recv.at[axis])
         for cc in range(2):
             parts = [rs[axis][cc, s].astype(F32) for s in range(4)]
-            first = BASE[axis] + cc * COLS[axis]
-            eo_ref[:, first : first + COLS[axis]] = (parts[0] + parts[1] + parts[2] + parts[3]).astype(BF16)
-
+            first = BACK_BASE[axis] + cc * BACK_COLS[axis]
+            eo_ref[:, first : first + BACK_COLS[axis]] = (parts[0] + parts[1] + parts[2] + parts[3]).astype(BF16)
+
+    give_sums = pltpu.make_async_copy(eo_ref, eo_hbm, give_sem.at[1])
+    give_sums.start()
     drain(dummy, meta_send)
     drain(kx.at[pl.ds(0, 128)], halo_send.at[0])
     drain(kx.at[pl.ds(0, 128)], halo_send.at[1])
@@ -445,7 +473,10 @@
     for axis in AXES:
         drain(pk[axis].at[pl.ds(0, 31)], pk_send.at[axis])
         drain(ret[axis].at[pl.ds(0, 31)], ret_send.at[axis])
-        drain(ag[axis].at[:, :, pl.ds(0, 112), :], rs_send.at[axis])
+        drain(out[axis].at[:, :, pl.ds(0, 112), :], rs_send.at[axis])
+        drain(ag[axis].at[:, :, pl.ds(0, 112), :], ag_send.at[axis])
+    give_mixed.wait()
+    give_sums.wait()
 
 
 def body(
@@ -453,11 +484,12 @@
     routes, route_weights, gate_weight, up_weight, down_weight,
 ):
     row_cos, row_sin, col_cos, col_sin, pairs = rope_tables()
-    vmem = pl.BlockSpec(memory_space=pltpu.VMEM)
     hbm = pl.BlockSpec(memory_space=pl.ANY)
     dma = pltpu.SemaphoreType.DMA
     V = pltpu.VMEM
     scratch = [
+        V((128, 2048), BF16), V((1, 2048), F32), V((4, 128), jnp.int32), V((4, 128), F32), V((256, 256), BF16),
+        V((64, 128), F32), V((64, 128), F32), V((256, 2048), BF16), V((128, 2048), BF16), dma((2,)),
         V((2048, 256), BF16), V((2304, 128), BF16), V((2304, 128), BF16),
         V((2304, 128), BF16), V((2304, 128), BF16), V((2304, 128), BF16),
         V((2048, 256), BF16), V((256, 2048), BF16),
@@ -467,18 +499,18 @@
         *[V((4, 2, 128, n), BF16) for n in COLS],
         *[V((32, 4, 16, n), BF16) for n in COLS],
         V((4, 4, 4, 16, 2048), BF16), V((512, 1024), BF16), V((4, 4, 4, 16, 2048), BF16),
-        *[V((32, 4, 16, n), BF16) for n in COLS],
-        V((3, 4, 256, 512), BF16),
-        *[V((2, 4, 128, n), BF16) for n in COLS],
+        *[V((32, 4, 16, n), BF16) for n in BACK_COLS],
+        V((3, 4, 256, 512), BF16), V((3, 4, 512, 256), BF16),
+        *[V((2, 4, 128, n), BF16) for n in BACK_COLS], *[V((4, 2, 128, n), BF16) for n in BACK_COLS],
         V((8, 128), F32), V((168, 128), F32),
-        dma((9,)), dma((4,)), dma((4,)), dma, dma, dma((3,)), dma((3,)),
-        dma((3,)), dma((3, 2)), dma, dma, dma((3,)), dma((3,)), dma((3,)), dma((3,)),
+        dma((16,)), dma((4,)), dma((4,)), dma, dma, dma((3,)), dma((3,)),
+        dma((3,)), dma((3, len(CHUNKS))), dma, dma, dma((3,)), dma((3,)), dma((3,)), dma((3,)),
     ]
     mixed, summed = pl.pallas_call(
         kernel,
         out_shape=(jax.ShapeDtypeStruct((256, 2048), BF16), jax.ShapeDtypeStruct((128, 2048), BF16)),
-        in_specs=[pl.BlockSpec(memory_space=pltpu.SMEM)] + [vmem] * 7 + [hbm] * 9,
-        out_specs=(vmem, vmem),
+        in_specs=[pl.BlockSpec(memory_space=pltpu.SMEM)] + [hbm] * 16,
+        out_specs=(hbm, hbm),
         scratch_shapes=scratch,
         compiler_params=pltpu.CompilerParams(
             collective_id=0, has_side_effects=True, vmem_limit_bytes=67043328

time: 119 us -> 109 us (0.916); the launches traced: 117 us -> 109 us
  Pallas kernels: 116 us -> 108 us
    pallas_call x1, Pallas kernels: 114 us -> 106 us  [body(): pl.pallas_call(kernel, out_shape=(jax.ShapeDtypeStruct((256, 2048), BF16)...]
where the time goes in v3:
time: 109 us
  Pallas kernels  108 us (99%)
    pallas_call x1, Pallas kernels, body(): pl.pallas_call(kernel, out_shape=(jax.ShapeDtypeStruct((256, 2048), BF16)...  106 us
    pallas_call x1, Pallas kernels, body(): pl.pallas_call(hand_over, out_shape=(jax.ShapeDtypeStruct((256, 2048), BF...  2.23 us

profile of v3, /device:TPU:1, one launch (start us, length us, event | category | flops | bytes accessed | tf_op | source)
XLA Modules:
  0.0 108.6 jit_solution(17407699723752203554)
XLA Ops:
  0.6 105.6 %layer.1 = (bf16[256,2048]{1,0:T(8,128)(2,1)}, bf16[128,2048]{1,0:T(8,128)(2,1)}) custom-call(f32[4]{0:T(128)} %sink_ref.1, bf16[128,2048]{1,0:T(8,128)(2,1)} %x_hbm.1, f32[1,2048]{1,0:T(1,128)} %bitcast.3, s32[4,128]{1,0:T(4,128)} %bitcast.4, f32[4,128]{1,0:T(4,128)} %bitcast.5, bf16[256,256]{1,0:T(8,128)(2,1)} %constant.10.clone.pairs_hbm, ...), custom_call_target="tpu_custom_call" | custom-call | tf_op jit(solution)/shard_map/layer/pallas_call | solution.py:509
  106.2 2.2 %finish.1 = (bf16[256,2048]{1,0:T(8,128)(2,1)}, bf16[128,2048]{1,0:T(8,128)(2,1)}) custom-call(bf16[256,2048]{1,0:T(8,128)(2,1)} %get-tuple-element.4.mixed, bf16[128,2048]{1,0:T(8,128)(2,1)} %get-tuple-element.5.summed), custom_call_target="tpu_custom_call" | custom-call | tf_op jit(solution)/shard_map/finish/pallas_call | solution.py:524

commit v4 on v3

--- a/solution.py
+++ b/solution.py
@@ -368,9 +368,9 @@
     drain(vx.at[pl.ds(2176, 128)], halo_recv.at[3])
     turn_keys(0, 0)
     turn_keys(17, 0)
-    lax.fori_loop(0, 4, attend_for, 0)
+    lax.fori_loop(0, 3, attend_for, 0)
     send_rows(messages(1, (0, 1, 2)))
-    lax.fori_loop(4, 8, attend_for, 0)
+    lax.fori_loop(3, 6, attend_for, 0)
 
     for copy in loads[5:8]:
         copy.wait()
@@ -420,6 +420,8 @@
         if 0 in steps:
             ret_y[self_at[0]] = prod[z, x, :, :, back_cols(0, c)]
             ret_x[self_at[1]] = prod[z, :, y, :, back_cols(1, c)]
+        if chunk == 0:
+            lax.fori_loop(6, 8, attend_for, 0)
         for zs in sources:
             ret_z[self_at[2], zs] = prod[zs, x, y, :, back_cols(2, c)]
 

time: 109 us -> 109 us (level)
  no operation moved by 1% of the time
where the time goes in v4:
time: 109 us; the launch traced here: 108 us
  Pallas kernels  108 us (99%)
    pallas_call x1, Pallas kernels, body(): pl.pallas_call(kernel, out_shape=(jax.ShapeDtypeStruct((256, 2048), BF16)...  105 us
    pallas_call x1, Pallas kernels, body(): pl.pallas_call(hand_over, out_shape=(jax.ShapeDtypeStruct((256, 2048), BF...  2.23 us

profile of v4, /device:TPU:1, one launch (start us, length us, event | category | flops | bytes accessed | tf_op | source)
XLA Modules:
  0.0 108.4 jit_solution(2915970820910577069)
XLA Ops:
  0.6 105.4 %layer.1 = (bf16[256,2048]{1,0:T(8,128)(2,1)}, bf16[128,2048]{1,0:T(8,128)(2,1)}) custom-call(f32[4]{0:T(128)} %sink_ref.1, bf16[128,2048]{1,0:T(8,128)(2,1)} %x_hbm.1, f32[1,2048]{1,0:T(1,128)} %bitcast.3, s32[4,128]{1,0:T(4,128)} %bitcast.4, f32[4,128]{1,0:T(4,128)} %bitcast.5, bf16[256,256]{1,0:T(8,128)(2,1)} %constant.10.clone.pairs_hbm, ...), custom_call_target="tpu_custom_call" | custom-call | tf_op jit(solution)/shard_map/layer/pallas_call | solution.py:511
  106.0 2.2 %finish.1 = (bf16[256,2048]{1,0:T(8,128)(2,1)}, bf16[128,2048]{1,0:T(8,128)(2,1)}) custom-call(bf16[256,2048]{1,0:T(8,128)(2,1)} %get-tuple-element.4.mixed, bf16[128,2048]{1,0:T(8,128)(2,1)} %get-tuple-element.5.summed), custom_call_target="tpu_custom_call" | custom-call | tf_op jit(solution)/shard_map/finish/pallas_call | solution.py:526
